TPU v7x, 32 devices: a whole 2x2x4 slice. The times are simulated.
32 devices in a mesh: sp: 16 (over z, y, x), tp: 2 (over core).
Axes of the slice: x: 2, y: 2, z: 4, core: 2. Of those that a mesh axis runs over, the one named last changes fastest.
Arguments:
- moe_input: bfloat16 [2048, 2048], P('sp'), may hold values from -6 to 6
- out_grad: bfloat16 [2048, 2048], P('sp'), may hold values from -8 to 8
- route_ids: int32 [2048, 2], P('sp'), may hold values from 0 to 7, all different within a row; in each aligned block of 128 rows (0 to 127, 128 to 255, ...) at most 48 rows name the same one
- route_weights: float32 [2048, 2], P('sp'), may hold values from 0.1 to 0.9
- gate_w: bfloat16 [16, 2048, 1792], P('sp', None, 'tp'), may hold values from -0.125 to 0.125
- up_w: bfloat16 [16, 2048, 1792], P('sp', None, 'tp'), may hold values from -0.125 to 0.125
- down_w: bfloat16 [16, 1792, 2048], P('sp', 'tp'), may hold values from -0.09375 to 0.09375
- mixer_out: bfloat16 [2048, 1024], P('sp', 'tp'), may hold values from -6 to 6
- out_weight: bfloat16 [1024, 2048], P('tp'), may hold values from -0.1875 to 0.1875
- queries: bfloat16 [2048, 512], P('sp', 'tp'), may hold values from -0.125 to 0.125
- keys: bfloat16 [2048, 512], P('sp', 'tp'), may hold values from -0.3125 to 0.3125
- values: bfloat16 [2048, 1024], P('sp', 'tp'), may hold values from -1.5 to 1.5
- log_decay: float32 [2048, 512], P('sp', 'tp'), may hold values from -0.1 to 0, as said below
- block_states: float32 [32, 8, 64, 128], P('sp', 'tp'), may hold values from -1.75 to 1.75
Outputs:
- grad_queries: bfloat16 [2048, 512], P('sp', 'tp')
- grad_keys: bfloat16 [2048, 512], P('sp', 'tp')
- grad_values: bfloat16 [2048, 1024], P('sp', 'tp')
- grad_decay: float32 [2048, 512], P('sp', 'tp')
- grad_out_weight: float32 [1024, 2048], P('tp', 'sp')
- grad_gate_w: bfloat16 [16, 2048, 1792], P('sp', None, 'tp')
- grad_up_w: bfloat16 [16, 2048, 1792], P('sp', None, 'tp')
- grad_down_w: bfloat16 [16, 1792, 2048], P('sp', 'tp')
Inputs may be any that keep to these rules, and one draw needn't show every extreme that they name: `route_ids`: each row names two different experts. In the rows of one index of sp no expert is named more than 48 times, and in every draw some expert is named exactly 48 times by the rows of some index of sp. `log_decay`: Negative.
All inputs are finite; a program needn't handle non-finite values.
Results may differ from a plain program's by a relative error of at most 0.013.
Values may be sent and summed in bfloat16 or wider, within the bound.
A program may use at most 128 MiB of HBM per device.

v0:
```python
import jax
import jax.numpy as jnp
from jax import lax
from jax.sharding import PartitionSpec as P

DK = 64
DV = 128
BLK = 64


PRECISE = lax.Precision.HIGHEST
ACROSS = (((1,), (1,)), ((), ()))
DOWNWARD = (((0,), (0,)), ((), ()))


def prefix(part, axis, combine, identity):
    count = lax.axis_size(axis)
    place = lax.axis_index(axis)
    ahead = count - 1 - place
    gathered = jax.tree.map(lambda a: lax.all_gather(a, axis), part)
    state = jax.tree.map(lambda a, e: jnp.zeros_like(a) + jnp.asarray(e, a.dtype), part, identity)

    def one(turn, state):
        source = count - 1 - turn
        return combine(
            state, jax.tree.map(lambda a: lax.dynamic_index_in_dim(a, source, 0, False), gathered)
        )

    return lax.fori_loop(0, ahead, one, state)


def block_back(carried, inputs):
    q_block, k_block, v_block, o_block, decay_block, state_in = inputs
    cumul = jnp.cumsum(decay_block, axis=0)
    block_total = cumul[-1]
    growth = jnp.exp(cumul)
    shrink = jnp.exp(-cumul)
    to_end = jnp.exp(block_total[None] - cumul)
    span_len = q_block.shape[0]
    causal = (jnp.arange(span_len)[:, None] >= jnp.arange(span_len)[None, :]).astype(jnp.float32)
    q_grow = q_block * growth
    k_shrink = k_block * shrink
    scores = jnp.einsum("thv,shv->hts", o_block, v_block, precision=PRECISE) * causal
    mutual = jnp.einsum("thd,shd->hts", q_grow, k_shrink, precision=PRECISE) * causal
    grad_q = growth * (
        jnp.einsum("thv,hdv->thd", o_block, state_in, precision=PRECISE)
        + jnp.einsum("hts,shd->thd", scores, k_shrink, precision=PRECISE)
    )
    grad_k = to_end * jnp.einsum(
        "hdv,shv->shd", carried, v_block, precision=PRECISE
    ) + shrink * jnp.einsum("hts,thd->shd", scores, q_grow, precision=PRECISE)
    grad_v = jnp.einsum("shd,hdv->shv", k_block * to_end, carried, precision=PRECISE) + jnp.einsum(
        "hts,thv->shv", mutual, o_block, precision=PRECISE
    )
    contrib = q_block * grad_q - k_block * grad_k
    carried = jnp.exp(block_total)[:, :, None] * carried + jnp.einsum(
        "thd,thv->hdv", q_grow, o_block, precision=PRECISE
    )
    return (carried, (grad_q, grad_k, grad_v, contrib))


def combine(earlier, latter):
    gain_early, sum_early, term_early, reach_early = earlier
    gain_late, sum_late, term_late, reach_late = latter
    return (
        gain_early * gain_late,
        gain_late[:, :, None] * sum_early + sum_late,
        term_early + term_late - jnp.sum(reach_late * sum_early, axis=2),
        reach_early + gain_early[:, :, None] * reach_late,
    )


def body(
    moe_input,
    out_grad,
    route_ids,
    route_weights,
    gate_w,
    up_w,
    down_w,
    mixer_out,
    out_weight,
    queries,
    keys,
    values,
    log_decay,
    block_states,
):
    sp_count = lax.axis_size("sp")
    experts = sp_count // 2
    tok_rows = moe_input.shape[0]
    model_width = moe_input.shape[1]
    capacity = 3 * tok_rows // experts
    flat_ids = route_ids.reshape(-1)
    one_hot = (flat_ids[:, None] == jnp.arange(experts, dtype=jnp.int32)[None, :]).astype(jnp.int32)
    earlier_count = jnp.sum(jnp.cumsum(one_hot, axis=0) * one_hot, axis=1) - 1
    slot_index = flat_ids * capacity + earlier_count
    dispatch = (
        jnp.arange(experts * capacity, dtype=jnp.int32)[:, None] == slot_index[None, :]
    ).astype(jnp.bfloat16)
    token_pick = jnp.sum(dispatch.reshape(experts * capacity, tok_rows, 2), axis=2)
    col_count = model_width // lax.axis_size("tp")
    col_start = lax.axis_index("tp") * col_count
    source_tokens = lax.dynamic_slice_in_dim(moe_input, col_start, col_count, 1)
    source_grads = lax.dynamic_slice_in_dim(out_grad, col_start, col_count, 1)
    send_width = source_tokens.shape[1]
    scaled = (route_weights[:, :, None] * source_grads[:, None, :].astype(jnp.float32)).astype(
        jnp.bfloat16
    )
    scaled = scaled.reshape(2 * tok_rows, send_width)
    token_send = jnp.dot(token_pick, source_tokens, preferred_element_type=jnp.float32).astype(
        jnp.bfloat16
    )
    grad_send = jnp.dot(dispatch, scaled, preferred_element_type=jnp.float32).astype(jnp.bfloat16)

    def spread(buffer):
        doubled = jnp.broadcast_to(
            buffer.reshape(experts, 1, capacity, send_width), (experts, 2, capacity, send_width)
        )
        return doubled.reshape(sp_count * capacity, send_width)

    arrived_tokens, arrived_grads = (
        lax.all_to_all(spread(token_send), "sp", split_axis=0, concat_axis=0, tiled=True),
        lax.all_to_all(spread(grad_send), "sp", split_axis=0, concat_axis=0, tiled=True),
    )
    arrived_tokens, arrived_grads = (
        lax.all_gather(arrived_tokens, "tp", axis=1, tiled=True),
        lax.all_gather(arrived_grads, "tp", axis=1, tiled=True),
    )
    gate_mat = gate_w[0]
    up_mat = up_w[0]
    down_mat = down_w[0]
    gate_pre = jnp.dot(arrived_tokens, gate_mat, preferred_element_type=jnp.float32)
    up_pre = jnp.dot(arrived_tokens, up_mat, preferred_element_type=jnp.float32)
    sigmoid_gate = jax.nn.sigmoid(gate_pre)
    hidden = (gate_pre * sigmoid_gate * up_pre).astype(jnp.bfloat16)
    d_hidden = lax.dot_general(arrived_grads, down_mat, ACROSS, preferred_element_type=jnp.float32)
    d_up = (d_hidden * gate_pre * sigmoid_gate).astype(jnp.bfloat16)
    d_gate = (d_hidden * up_pre * sigmoid_gate * (1.0 + gate_pre * (1.0 - sigmoid_gate))).astype(
        jnp.bfloat16
    )
    grad_down = lax.dot_general(
        hidden, arrived_grads, DOWNWARD, preferred_element_type=jnp.float32
    ).astype(jnp.bfloat16)
    grad_gate = lax.dot_general(
        arrived_tokens, d_gate, DOWNWARD, preferred_element_type=jnp.float32
    ).astype(jnp.bfloat16)
    grad_up = lax.dot_general(
        arrived_tokens, d_up, DOWNWARD, preferred_element_type=jnp.float32
    ).astype(jnp.bfloat16)
    partial_value = lax.dot_general(
        d_gate, gate_mat, ACROSS, preferred_element_type=jnp.float32
    ) + lax.dot_general(d_up, up_mat, ACROSS, preferred_element_type=jnp.float32)
    half_grad = lax.psum_scatter(
        partial_value.astype(jnp.bfloat16), "tp", scatter_dimension=1, tiled=True
    )
    returned = lax.all_to_all(half_grad, "sp", split_axis=0, concat_axis=0, tiled=True)
    pick_both = jnp.broadcast_to(
        token_pick.reshape(experts, 1, capacity, tok_rows), (experts, 2, capacity, tok_rows)
    ).reshape(sp_count * capacity, tok_rows)
    moe_grad = lax.dot_general(pick_both, returned, DOWNWARD, preferred_element_type=jnp.float32)
    grad_mid = (source_grads.astype(jnp.float32) + moe_grad).astype(jnp.bfloat16)
    grad_mid = lax.all_gather(grad_mid, "tp", axis=1, tiled=True)
    grad_out_weight = lax.psum_scatter(
        lax.dot_general(grad_mid, mixer_out, DOWNWARD, preferred_element_type=jnp.float32),
        "sp",
        scatter_dimension=0,
        tiled=True,
    ).T
    grad_mixed = lax.dot_general(
        grad_mid, out_weight, ACROSS, preferred_element_type=jnp.float32
    ).astype(jnp.bfloat16)
    heads_local = queries.shape[1] // DK
    blocks = tok_rows // BLK

    def shaped(array, depth):
        return array.astype(jnp.float32).reshape(blocks, BLK, heads_local, depth)

    q_blocks = shaped(queries, DK)
    k_blocks = shaped(keys, DK)
    v_blocks = shaped(values, DV)
    decay_blocks = shaped(log_decay, DK)
    inputs = (q_blocks, k_blocks, v_blocks, shaped(grad_mixed, DV), decay_blocks, block_states)
    zero_state = jnp.zeros((heads_local, DK, DV), jnp.float32)
    local_sum, (grad_q, grad_k, grad_v, contrib) = lax.scan(
        block_back, zero_state, inputs, reverse=True
    )
    cumul = jnp.cumsum(decay_blocks, axis=1)
    totals = cumul[:, -1]
    offsets = jnp.cumsum(totals, axis=0) - totals
    position = cumul + offsets[:, None]
    device_total = jnp.sum(totals, axis=0)
    fade_out = jnp.exp(device_total[None, None] - position)
    k_fade = k_blocks * fade_out
    reach_sum = jnp.einsum("nshd,nshv->hdv", k_fade, v_blocks, precision=PRECISE)
    identity = (
        jnp.ones((heads_local, DK), jnp.float32),
        jnp.zeros((heads_local, DK, DV), jnp.float32),
        jnp.zeros((heads_local, DK), jnp.float32),
        jnp.zeros((heads_local, DK, DV), jnp.float32),
    )
    scanned = prefix(
        (jnp.exp(device_total), local_sum, jnp.sum(contrib, axis=(0, 1)), reach_sum),
        "sp",
        combine,
        identity,
    )
    from_right = scanned[1]
    right_terms = scanned[2]
    key_part = jnp.einsum("nshv,hdv->nshd", v_blocks, from_right, precision=PRECISE)
    grad_k = grad_k + fade_out * key_part
    grad_v = grad_v + jnp.einsum("nshd,hdv->nshv", k_fade, from_right, precision=PRECISE)
    contrib = (contrib - k_fade * key_part).reshape(tok_rows, heads_local * DK)
    grad_decay = jnp.flip(jnp.cumsum(jnp.flip(contrib, 0), axis=0), 0) + right_terms.reshape(1, -1)
    return (
        grad_q.reshape(tok_rows, heads_local * DK).astype(jnp.bfloat16),
        grad_k.reshape(tok_rows, heads_local * DK).astype(jnp.bfloat16),
        grad_v.reshape(tok_rows, heads_local * DV).astype(jnp.bfloat16),
        grad_decay,
        grad_out_weight,
        grad_gate[None],
        grad_up[None],
        grad_down[None],
    )


def solution(mesh):
    placed = (
        P("sp", None),
        P("sp", None),
        P("sp", None),
        P("sp", None),
        P("sp", None, "tp"),
        P("sp", None, "tp"),
        P("sp", "tp", None),
        P("sp", "tp"),
        P("tp", None),
        P("sp", "tp"),
        P("sp", "tp"),
        P("sp", "tp"),
        P("sp", "tp"),
        P("sp", "tp", None, None),
    )
    return jax.shard_map(
        body,
        mesh=mesh,
        in_specs=placed,
        out_specs=(
            P("sp", "tp"),
            P("sp", "tp"),
            P("sp", "tp"),
            P("sp", "tp"),
            P("tp", "sp"),
            P("sp", None, "tp"),
            P("sp", None, "tp"),
            P("sp", "tp", None),
        ),
        check_vma=False,
    )
```

profile of v0, /device:TPU:0, one launch (start us, length us, event | category | flops | bytes accessed | tf_op | source)
XLA Modules:
  0.0 389.1 jit_solution(16481995954714678232)
XLA Ops:
  13.9 8.4 %all-to-all-start.1 = ((bf16[16,48,1024]{2,1,0:T(8,128)(2,1)}), bf16[16,48,1024]{2,1,0:T(8,128)(2,1)}, u32[]{:S(2)}, u32[]{:S(2)}) async-start(bf16[16,48,1024]{2,1,0:T(8,128)(2,1)} %bitcast.248), calls=%async_computation.1 | async-start | bytes 3145728 | tf_op jit(solution)/shard_map/all_to_all | solution.py:123
  23.8 1.9 mul.244
  26.0 30.5 %all-to-all-done.1 = bf16[16,48,1024]{2,1,0:T(8,128)(2,1)} async-done(((bf16[16,48,1024]{2,1,0:T(8,128)(2,1)}), bf16[16,48,1024]{2,1,0:T(8,128)(2,1)}, u32[]{:S(2)}, u32[]{:S(2)}) %all-to-all-start.1) | async-done | bytes 1572896 | tf_op jit(solution)/shard_map/all_to_all | solution.py:123
  57.2 44.5 %all_to_all.36 = bf16[16,48,1024]{2,1,0:T(8,128)(2,1)} all-to-all(bf16[16,48,1024]{2,1,0:T(8,128)(2,1)S(1)} %bitcast.249), channel_id=1, replica_groups=mesh['sp'=16,'tp'=2] {'sp'}, dimensions={0} | all-to-all | bytes 3145728 | tf_op jit(solution)/shard_map/all_to_all | solution.py:124
  102.0 8.2 %fusion.32 = f32[768,896]{1,0:T(8,128)} fusion(bf16[768,2048]{1,0:T(8,128)(2,1)} %all-gather.13.cloned.1.call-done, bf16[1,2048,896]{2,1,0:T(8,128)(2,1)} %param.22), kind=kOutput, calls=%fused_computation.63 | convolution fusion | flops 2818572288 | bytes 9568256 | tf_op jit(solution)/shard_map/dot_general | solution.py:133
  110.2 4.9 %fusion.36 = f32[768,896]{1,0:T(8,128)} fusion(bf16[768,2048]{1,0:T(8,128)(2,1)S(1)} %copy-done.20, bf16[1,2048,896]{2,1,0:T(8,128)(2,1)S(1)} %copy-done.18), kind=kOutput, calls=%fused_computation.67 | convolution fusion | flops 2818572288 | bytes 9568256 | tf_op jit(solution)/shard_map/dot_general | solution.py:134
  115.1 8.8 %multiply_convert_fusion.1 = (bf16[768,896]{1,0:T(8,128)(2,1)S(1)}, bf16[768,896]{1,0:T(8,128)(2,1)S(1)}) fusion(f32[768,896]{1,0:T(8,128)} %fusion.32, f32[768,896]{1,0:T(8,128)} %fusion.36, bf16[768,2048]{1,0:T(8,128)(2,1)} %all-gather.11.cloned.1.call-done, bf16[1,896,2048]{2,1,0:T(8,128)(2,1)} %param.24), kind=kOutput, calls=%fused_computation.75 | convolution fusion | flops 2827517952 | bytes 15073280 | tf_op jit(solution)/shard_map/dot_general | solution.py:137
  124.0 3.4 fusion.30
  127.5 4.8 %add_convert_fusion = bf16[768,2048]{1,0:T(8,128)(2,1)} fusion(f32[768,2048]{1,0:T(8,128)S(1)} %fusion.30, bf16[768,896]{1,0:T(8,128)(2,1)S(1)} %get-tuple-element.574, bf16[1,2048,896]{2,1,0:T(8,128)(2,1)S(1)} %copy-done.19), kind=kOutput, calls=%fused_computation.60 | convolution fusion | flops 2821718016 | bytes 14483456 | tf_op jit(solution)/shard_map/dot_general | solution.py:153
  132.3 9.5 %reduce-scatter.3.cloned.1.call-done = bf16[768,1024]{1,0:T(8,128)(2,1)} async-done(((bf16[768,2048]{1,0:T(8,128)(2,1)}), bf16[768,1024]{1,0:T(8,128)(2,1)}) %reduce-scatter.3.cloned.1.call-update) | async-done | bytes 1572880 | tf_op jit(solution)/shard_map/reduce_scatter | solution.py:154
  141.8 6.9 %all-to-all-start.2 = ((bf16[16,48,1024]{2,1,0:T(8,128)(2,1)}), bf16[16,48,1024]{2,1,0:T(8,128)(2,1)}, u32[]{:S(2)}, u32[]{:S(2)}) async-start(bf16[16,48,1024]{2,1,0:T(8,128)(2,1)} %bitcast.252), calls=%async_computation.3 | async-start | bytes 3145728 | tf_op jit(solution)/shard_map/all_to_all | solution.py:157
  154.2 31.7 %all-to-all-done.2 = bf16[16,48,1024]{2,1,0:T(8,128)(2,1)} async-done(((bf16[16,48,1024]{2,1,0:T(8,128)(2,1)}), bf16[16,48,1024]{2,1,0:T(8,128)(2,1)}, u32[]{:S(2)}, u32[]{:S(2)}) %all-to-all-start.2) | async-done | bytes 1572896 | tf_op jit(solution)/shard_map/all_to_all | solution.py:157
  186.8 1.8 fusion.43
  188.6 2.2 all_gather.33
  194.1 15.4 %while.41 = (s32[]{:T(128)}, f32[4,64,128]{2,1,0:T(8,128)S(1)}, bf16[2,64,4,64]{1,3,2,0:T(8,128)(2,1)}, f32[2,64,4,64]{1,3,0,2:T(8,128)}, f32[2,64,4,128]{3,1,0,...) while((s32[]{:T(128)}, f32[4,64,128]{2,1,0:T(8,128)S(1)}, ...), condition=%wide.region_7.8_spmd.clone, body=%wide.region_5.7_spmd.clone.sunk | while | flops 190324736 | bytes 5891257 | solution.py:185
  210.2 3.6 fusion.62
  214.0 44.2 %all-gather.4 = f32[16,4,64]{2,1,0:T(4,128)S(1)} all-gather(f32[1,4,64]{2,1,0:T(4,128)S(1)} %exponential_bitcast_fusion), channel_id=2, replica_groups=mesh['sp'=16,'tp'=2] {'sp'}, dimensions={0}, use_global_device_ids=true | all-gather | bytes 17408 | tf_op jit(solution)/shard_map/all_gather | solution.py:20
  258.3 7.7 %convert_bitcast_fusion.1 = bf16[1,2048,896]{2,1,0:T(8,128)(2,1)} fusion(bf16[768,2048]{1,0:T(8,128)(2,1)} %all-gather.13.cloned.1.call-done, bf16[768,896]{1,0:T(8,128)(2,1)} %copy-done.27), kind=kOutput, calls=%fused_computation.72 | convolution fusion | flops 2820407296 | bytes 8192000 | tf_op jit(solution)/shard_map/dot_general | solution.py:148
  266.0 4.9 %convert_bitcast_fusion.2 = bf16[1,2048,896]{2,1,0:T(8,128)(2,1)} fusion(bf16[768,2048]{1,0:T(8,128)(2,1)S(1)} %copy-done.21, bf16[768,896]{1,0:T(8,128)(2,1)S(1)} %copy-done.24), kind=kOutput, calls=%fused_computation.73 | convolution fusion | flops 2820407296 | bytes 8192000 | tf_op jit(solution)/shard_map/dot_general | solution.py:145
  271.0 4.7 %convert_bitcast_fusion = bf16[1,896,2048]{2,1,0:T(8,128)(2,1)} fusion(bf16[768,2048]{1,0:T(8,128)(2,1)S(1)} %copy-done.22, f32[768,896]{1,0:T(8,128)S(1)} %copy-done.26, f32[768,896]{1,0:T(8,128)S(1)} %copy-done.25), kind=kOutput, calls=%fused_computation.71 | convolution fusion | flops 2824536064 | bytes 12320768 | tf_op jit(solution)/shard_map/dot_general | solution.py:142
  276.7 36.1 %all-gather.5 = f32[16,4,64]{2,1,0:T(4,128)S(1)} all-gather(f32[1,4,64]{2,1,0:T(4,128)S(1)} %bitcast.262), channel_id=4, replica_groups=mesh['sp'=16,'tp'=2] {'sp'}, dimensions={0}, use_global_device_ids=true | all-gather | bytes 17408 | tf_op jit(solution)/shard_map/all_gather | solution.py:20
  312.9 18.1 %while.40 = (s32[]{:T(128)}, f32[4,64,128]{2,1,0:T(8,128)S(1)}, f32[4,64]{1,0:T(4,128)S(1)}, s32[]{:T(128)}, f32[16,4,64]{2,1,0:T(4,128)S(1)}, /*index=5*/f32[16...) while((s32[]{:T(128)}, f32[4,64,128]{2,1,0:T(8,128)S(1)}, ...), condition=%wide.region_14.15_spmd, body=%wide.region_12.14_spmd.sunk | while | flops 131334 | bytes 532655 | solution.py:29
  331.1 2.3 copy_subtract_fusion
  338.9 41.1 %reduce-scatter.5.cloned.1.call-done = f32[128,512]{1,0:T(8,128)} async-done(((f32[2048,512]{1,0:T(8,128)}), f32[128,512]{1,0:T(8,128)}) %reduce-scatter.5.cloned.1.call-update) | async-done | bytes 262160 | tf_op jit(solution)/shard_map/reduce_scatter | solution.py:164
  (219 shorter events, 59.8 us)
Async XLA Ops:
  8.0 182.8 %copy-start = (bf16[512,2048]{1,0:T(8,128)(2,1)S(1)}, bf16[512,2048]{1,0:T(8,128)(2,1)}, u32[]{:S(2)}) copy-start(bf16[512,2048]{1,0:T(8,128)(2,1)} %param.26) | copy-start | bytes 6291460
  12.5 9.8 %copy-start.11 = (bf16[128,2048]{1,0:T(8,128)(2,1)S(1)}, bf16[128,2048]{1,0:T(8,128)(2,1)}, u32[]{:S(2)}) copy-start(bf16[128,2048]{1,0:T(8,128)(2,1)} %param.19) | copy-start | bytes 1572868
  13.9 42.6 %all-to-all-start.1 = ((bf16[16,48,1024]{2,1,0:T(8,128)(2,1)}), bf16[16,48,1024]{2,1,0:T(8,128)(2,1)}, u32[]{:S(2)}, u32[]{:S(2)}) async-start(bf16[16,48,1024]{2,1,0:T(8,128)(2,1)} %bitcast.248), calls=%async_computation.1 | async-start | bytes 3145728 | tf_op jit(solution)/shard_map/all_to_all | solution.py:123
  22.3 79.7 %all-gather.13.cloned.1.call-start = ((), (), s32[]{:S(2)}) async-start(), calls=%async_computation.6 | async-start | bytes 4718592 | tf_op jit(solution)/shard_map/all_gather | solution.py:127
  56.5 58.6 %all-gather.11.cloned.1.call-start = ((), (), s32[]{:S(2)}) async-start(), calls=%async_computation.5 | async-start | bytes 4718592 | tf_op jit(solution)/shard_map/all_gather | solution.py:128
  101.8 40.0 %reduce-scatter.3.cloned.1.call-start = ((), (), s32[]{:S(2)}) async-start(), calls=%async_computation.7 | async-start | bytes 4718592 | tf_op jit(solution)/shard_map/reduce_scatter | solution.py:154
  102.0 8.2 %copy-start.18 = (bf16[1,2048,896]{2,1,0:T(8,128)(2,1)S(1)}, bf16[1,2048,896]{2,1,0:T(8,128)(2,1)}, u32[]{:S(2)}) copy-start(bf16[1,2048,896]{2,1,0:T(8,128)(2,1)} %param.23) | copy-start | bytes 11010052
  102.0 8.2 %copy-start.20 = (bf16[768,2048]{1,0:T(8,128)(2,1)S(1)}, bf16[768,2048]{1,0:T(8,128)(2,1)}, u32[]{:S(2)}) copy-start(bf16[768,2048]{1,0:T(8,128)(2,1)} %all-gather.13.cloned.1.call-done) | copy-start | bytes 9437188
  115.1 8.8 %copy-start.17 = (bf16[1,2048,896]{2,1,0:T(8,128)(2,1)S(1)}, bf16[1,2048,896]{2,1,0:T(8,128)(2,1)}, u32[]{:S(2)}) copy-start(bf16[1,2048,896]{2,1,0:T(8,128)(2,1)} %param.22) | copy-start | bytes 11010052
  132.3 16.5 %copy-start.14 = (bf16[128,512]{1,0:T(8,128)(2,1)S(1)}, bf16[128,512]{1,0:T(8,128)(2,1)}, u32[]{:S(2)}) copy-start(bf16[128,512]{1,0:T(8,128)(2,1)} %param.29) | copy-start | bytes 393220
  132.3 16.6 %copy-start.13 = (f32[128,256]{1,0:T(8,128)S(1)}, f32[128,256]{1,0:T(8,128)}, u32[]{:S(2)}) copy-start(f32[128,256]{1,0:T(8,128)} %param.30) | copy-start | bytes 393220
  132.3 16.7 %copy-start.15 = (bf16[128,256]{1,0:T(8,128)(2,1)S(1)}, bf16[128,256]{1,0:T(8,128)(2,1)}, u32[]{:S(2)}) copy-start(bf16[128,256]{1,0:T(8,128)(2,1)} %param.28) | copy-start | bytes 196612
  141.8 44.0 %all-to-all-start.2 = ((bf16[16,48,1024]{2,1,0:T(8,128)(2,1)}), bf16[16,48,1024]{2,1,0:T(8,128)(2,1)}, u32[]{:S(2)}, u32[]{:S(2)}) async-start(bf16[16,48,1024]{2,1,0:T(8,128)(2,1)} %bitcast.252), calls=%async_computation.3 | async-start | bytes 3145728 | tf_op jit(solution)/shard_map/all_to_all | solution.py:157
  148.8 164.1 %all-gather.17.cloned.1.call-start = ((), (), s32[]{:S(2)}) async-start(), calls=%async_computation.10 | async-start | bytes 2228224 | tf_op jit(solution)/shard_map/all_gather | solution.py:20
  148.9 37.9 %copy-start.7 = (bf16[2,64,4,128]{3,2,1,0:T(4,128)(2,1)}, bf16[2,64,4,128]{3,2,1,0:T(4,128)(2,1)S(1)}, u32[]{:S(2)}) copy-start(bf16[2,64,4,128]{3,2,1,0:T(4,128)(2,1)S(1)} %reshape.166) | copy-start | bytes 393220
  150.8 162.1 %all-gather.15.cloned.1.call-start = ((), (), s32[]{:S(2)}) async-start(), calls=%async_computation.9 | async-start | bytes 2228224 | tf_op jit(solution)/shard_map/all_gather | solution.py:20
  209.5 66.1 %copy-start.5 = (f32[2,64,4,64]{1,3,2,0:T(8,128)}, f32[2,64,4,64]{1,3,2,0:T(8,128)S(1)}, u32[]{:S(2)}) copy-start(f32[2,64,4,64]{1,3,2,0:T(8,128)S(1)} %get-tuple-element.382) | copy-start | bytes 393220
  210.2 169.8 %reduce-scatter.5.cloned.1.call-start = ((), (), s32[]{:S(2)}) async-start(), calls=%async_computation.8 | async-start | bytes 4456448 | tf_op jit(solution)/shard_map/reduce_scatter | solution.py:164
  258.3 7.8 %copy-start.21 = (bf16[768,2048]{1,0:T(8,128)(2,1)S(1)}, bf16[768,2048]{1,0:T(8,128)(2,1)}, u32[]{:S(2)}) copy-start(bf16[768,2048]{1,0:T(8,128)(2,1)} %all-gather.13.cloned.1.call-done) | copy-start | bytes 9437188
  258.3 7.8 %copy-start.24 = (bf16[768,896]{1,0:T(8,128)(2,1)S(1)}, bf16[768,896]{1,0:T(8,128)(2,1)}, u32[]{:S(2)}) copy-start(bf16[768,896]{1,0:T(8,128)(2,1)} %copy-done.23) | copy-start | bytes 4128772
  275.7 55.4 %copy-start.4 = (f32[2,64,4,64]{1,3,0,2:T(8,128)S(1)}, f32[2,64,4,64]{1,3,0,2:T(8,128)}, u32[]{:S(2)}) copy-start(f32[2,64,4,64]{1,3,0,2:T(8,128)} %copy-done.3) | copy-start | bytes 393220
  275.7 55.4 %copy-start.8 = (bf16[2,64,4,128]{3,2,1,0:T(4,128)(2,1)S(1)}, bf16[2,64,4,128]{3,2,1,0:T(4,128)(2,1)}, u32[]{:S(2)}) copy-start(bf16[2,64,4,128]{3,2,1,0:T(4,128)(2,1)} %copy-done.7) | copy-start | bytes 393220
  275.8 55.3 %copy-start.6 = (f32[2,64,4,64]{1,3,2,0:T(8,128)S(1)}, f32[2,64,4,64]{1,3,2,0:T(8,128)}, u32[]{:S(2)}) copy-start(f32[2,64,4,64]{1,3,2,0:T(8,128)} %copy-done.5) | copy-start | bytes 393220
  331.1 50.7 %copy-start.1 = (bf16[512,2048]{1,0:T(8,128)(2,1)S(1)}, bf16[512,2048]{1,0:T(8,128)(2,1)}, u32[]{:S(2)}) copy-start(bf16[512,2048]{1,0:T(8,128)(2,1)} %param.26) | copy-start | bytes 6291460
  (12 other events, 42.9 us)
Sparse Core Ops, SparseCore 0:
  56.6 14.2 all-gather.12
  101.9 10.4 all-gather.10
  132.4 9.3 reduce-scatter.2
Sparse Core Ops, SparseCore 1:
  152.0 68.7 all-gather.16
  223.5 59.3 all-gather.14
  285.0 94.9 reduce-scatter.4
where the time goes:
time: 390 us; the launch traced here: 389 us
  blocking collectives  127 us (33%)
  waiting for transfers between devices  113 us (29%)
  matrix products  69.2 us (18%)
  local copies, waits for them, and re-layouts  24.4 us (6%)
  other arithmetic  22.7 us (6%)
  starting transfers between devices  16 us (4%)
  between operations  16 us (4%)
    all_gather x2, blocking collectives, prefix(): gathered = jax.tree.map(lambda a: lax.all_gather(a, axis), part)  80.4 us
    all_to_all x1, blocking collectives, body(): lax.all_to_all(spread(grad_send), 'sp', split_axis=0, concat_axis=0, tile...  44.5 us
    reduce_scatter x1, waiting for transfers between devices, body(): lax.psum_scatter(lax.dot_general(grad_mid, mixer_out, DOWNWARD, preferred...  41.1 us
    all_to_all x1, waiting for transfers between devices, body(): lax.all_to_all(half_grad, 'sp', split_axis=0, concat_axis=0, tiled=True)  31.7 us
    all_to_all x1, waiting for transfers between devices, body(): lax.all_to_all(spread(token_send), 'sp', split_axis=0, concat_axis=0, til...  30.5 us
    reduce_sum x15, other arithmetic, combine(): jnp.sum(reach_late * sum_early, axis=2)  17.1 us
    reduce_scatter x1, waiting for transfers between devices, body(): lax.psum_scatter(partial_value.astype(jnp.bfloat16), 'tp', scatter_dimens...  9.49 us
    dot_general x1, matrix products, body(): lax.dot_general(arrived_grads, down_mat, ACROSS, preferred_element_type=j...  8.79 us
  transfers between devices with their start and end apart: 8, of which 4 were waited for; matrix products, arithmetic and copies ran while one was open for 23% of the time, Pallas kernels for 0%

commit v1 on v0

--- a/solution.py
+++ b/solution.py
@@ -1,7 +1,14 @@
+import functools
+
 import jax
 import jax.numpy as jnp
 from jax import lax
-from jax.sharding import PartitionSpec as P
+from jax.experimental import pallas as pl
+from jax.experimental.pallas import tpu as pltpu
+from jax.sharding import Mesh, PartitionSpec as P
+
+MESH = pl.DeviceIdType.MESH
+SP = ("ep", "pair")
 
 DK = 64
 DV = 128
@@ -13,20 +20,222 @@
 DOWNWARD = (((0,), (0,)), ((), ()))
 
 
-def prefix(part, axis, combine, identity):
-    count = lax.axis_size(axis)
-    place = lax.axis_index(axis)
-    ahead = count - 1 - place
-    gathered = jax.tree.map(lambda a: lax.all_gather(a, axis), part)
-    state = jax.tree.map(lambda a, e: jnp.zeros_like(a) + jnp.asarray(e, a.dtype), part, identity)
-
-    def one(turn, state):
-        source = count - 1 - turn
-        return combine(
-            state, jax.tree.map(lambda a: lax.dynamic_index_in_dim(a, source, 0, False), gathered)
-        )
-
-    return lax.fori_loop(0, ahead, one, state)
+def sp_size():
+    return lax.axis_size("ep") * lax.axis_size("pair")
+
+
+def sp_index():
+    return lax.axis_index("ep") * lax.axis_size("pair") + lax.axis_index("pair")
+
+
+def dispatch_kernel(
+    experts, width, tok_send, grad_send, tok_out, grad_out,
+    local_sem, direct_send, direct_recv, pair_send, pair_recv, core_send, core_recv,
+):
+    e, p, t = lax.axis_index("ep"), lax.axis_index("pair"), lax.axis_index("tp")
+    barrier = pltpu.get_barrier_semaphore()
+    for k in range(1, experts):
+        pl.semaphore_signal(
+            barrier, inc=1, device_id=(lax.rem(e + k, experts), p, t), device_id_type=MESH
+        )
+    pl.semaphore_signal(barrier, inc=1, device_id=(e, 1 - p, t), device_id_type=MESH)
+    pl.semaphore_signal(barrier, inc=1, device_id=(e, p, 1 - t), device_id_type=MESH)
+    pl.semaphore_wait(barrier, experts + 1)
+    columns = pl.ds(pl.multiple_of(t * width, 128), width)
+    sends, outs = (tok_send, grad_send), (tok_out, grad_out)
+
+    def direct(a, k):
+        if k == 0:
+            return pltpu.make_async_copy(
+                sends[a].at[e], outs[a].at[p, e, :, columns], local_sem.at[a]
+            )
+        dest = lax.rem(e + k, experts)
+        return pltpu.make_async_remote_copy(
+            src_ref=sends[a].at[dest],
+            dst_ref=outs[a].at[p, e, :, columns],
+            send_sem=direct_send.at[a, k],
+            recv_sem=direct_recv.at[a, k],
+            device_id=(dest, p, t),
+            device_id_type=MESH,
+        )
+
+    def passed(a, k, which, to_pair):
+        source = lax.rem(e - k + experts, experts)
+        place = outs[a].at[p if which == 0 else 1 - p, source, :, columns]
+        return pltpu.make_async_remote_copy(
+            src_ref=place,
+            dst_ref=place,
+            send_sem=pair_send.at[a, k] if to_pair else core_send.at[a, which, k],
+            recv_sem=pair_recv.at[a, k] if to_pair else core_recv.at[a, which, k],
+            device_id=(e, 1 - p, t) if to_pair else (e, p, 1 - t),
+            device_id_type=MESH,
+        )
+
+    def landed_direct(a, k):
+        if k == 0:
+            direct(a, 0).wait()
+            return
+        source = lax.rem(e - k + experts, experts)
+        place = outs[a].at[p, source, :, columns]
+        pltpu.make_async_remote_copy(
+            src_ref=place, dst_ref=place, send_sem=direct_send.at[a, k],
+            recv_sem=direct_recv.at[a, k], device_id=(source, p, t), device_id_type=MESH,
+        ).wait_recv()
+
+    def landed_passed(a, k, which, from_pair):
+        source = lax.rem(e - k + experts, experts)
+        own = p if which == 0 else 1 - p
+        if from_pair:
+            place = outs[a].at[1 - p, source, :, columns]
+            sems = (pair_send.at[a, k], pair_recv.at[a, k])
+        else:
+            other = pl.ds(pl.multiple_of((1 - t) * width, 128), width)
+            place = outs[a].at[own, source, :, other]
+            sems = (core_send.at[a, which, k], core_recv.at[a, which, k])
+        pltpu.make_async_remote_copy(
+            src_ref=place, dst_ref=place, send_sem=sems[0], recv_sem=sems[1],
+            device_id=(e, 1 - p, t), device_id_type=MESH,
+        ).wait_recv()
+
+    for a in range(2):
+        for k in range(experts):
+            direct(a, k).start()
+    steps = [(a, k) for a in range(2) for k in range(experts)]
+    lag = 2
+    for i in range(len(steps) + lag):
+        if i < len(steps):
+            a, k = steps[i]
+            landed_direct(a, k)
+            passed(a, k, 0, True).start()
+            passed(a, k, 0, False).start()
+        if i >= lag:
+            a, k = steps[i - lag]
+            landed_passed(a, k, 1, True)
+            passed(a, k, 1, False).start()
+    for a, k in steps:
+        for which in range(2):
+            landed_passed(a, k, which, False)
+    for a, k in steps:
+        if k:
+            direct(a, k).wait_send()
+        passed(a, k, 0, True).wait_send()
+        passed(a, k, 0, False).wait_send()
+        passed(a, k, 1, False).wait_send()
+
+
+def dispatch_rows(token_send, grad_send):
+    experts, capacity, width = token_send.shape
+    out = jax.ShapeDtypeStruct((2, experts, capacity, 2 * width), token_send.dtype)
+    vmem = pl.BlockSpec(memory_space=pltpu.VMEM)
+    dma = pltpu.SemaphoreType.DMA
+    return pl.pallas_call(
+        functools.partial(dispatch_kernel, experts, width),
+        out_shape=(out, out),
+        in_specs=[vmem, vmem],
+        out_specs=(vmem, vmem),
+        scratch_shapes=[
+            dma((2,)),
+            dma((2, experts)),
+            dma((2, experts)),
+            dma((2, experts)),
+            dma((2, experts)),
+            dma((2, 2, experts)),
+            dma((2, 2, experts)),
+        ],
+        compiler_params=pltpu.CompilerParams(collective_id=0, has_side_effects=True),
+        name="dispatch_rows",
+    )(token_send, grad_send)
+
+
+def suffix_kernel(count, rows, state, out, held, result, local_sem, go_send, go_recv, back_send, back_recv):
+    me = sp_index()
+    t = lax.axis_index("tp")
+
+    def place(i):
+        return (lax.div(i, 2), lax.rem(i, 2), t)
+
+    barrier = pltpu.get_barrier_semaphore()
+    for k in range(1, count):
+        pl.semaphore_signal(
+            barrier, inc=1, device_id=place(lax.rem(me + k, count)), device_id_type=MESH
+        )
+    pl.semaphore_wait(barrier, count - 1)
+
+    def go(k):
+        dest = lax.rem(me + k, count)
+        if k == 0:
+            return pltpu.make_async_copy(state.at[me], held.at[me], local_sem.at[0])
+        return pltpu.make_async_remote_copy(
+            src_ref=state.at[dest], dst_ref=held.at[me], send_sem=go_send.at[k],
+            recv_sem=go_recv.at[k], device_id=place(dest), device_id_type=MESH,
+        )
+
+    def back(k):
+        dest = lax.rem(me + k, count)
+        if k == 0:
+            return pltpu.make_async_copy(result.at[me], out.at[me], local_sem.at[1])
+        return pltpu.make_async_remote_copy(
+            src_ref=result.at[dest], dst_ref=out.at[me], send_sem=back_send.at[k],
+            recv_sem=back_recv.at[k], device_id=place(dest), device_id_type=MESH,
+        )
+
+    def landed(ref, sends, recvs, k):
+        source = lax.rem(me - k + count, count)
+        pltpu.make_async_remote_copy(
+            src_ref=ref.at[source], dst_ref=ref.at[source], send_sem=sends.at[k],
+            recv_sem=recvs.at[k], device_id=place(source), device_id_type=MESH,
+        ).wait_recv()
+
+    for k in range(count):
+        go(k).start()
+    go(0).wait()
+    for k in range(1, count):
+        landed(held, go_send, go_recv, k)
+    total = jnp.zeros((rows, state.shape[-1]), jnp.float32)
+    for i in range(count - 1, -1, -1):
+        result[i] = total
+        total = held[i, 1] * total + held[i, 0]
+    for k in range(count):
+        back(k).start()
+    back(0).wait()
+    for k in range(1, count):
+        landed(out, back_send, back_recv, k)
+    for k in range(1, count):
+        go(k).wait_send()
+        back(k).wait_send()
+
+
+def suffix_states(gain, local_sum):
+    count = sp_size()
+    heads, dk, dv = local_sum.shape
+    rows = heads * dk // count
+    packed = jnp.stack(
+        [
+            local_sum.reshape(count, rows, dv),
+            jnp.broadcast_to(gain[:, :, None], local_sum.shape).reshape(count, rows, dv),
+        ],
+        axis=1,
+    )
+    vmem = pl.BlockSpec(memory_space=pltpu.VMEM)
+    dma = pltpu.SemaphoreType.DMA
+    out = pl.pallas_call(
+        functools.partial(suffix_kernel, count, rows),
+        out_shape=jax.ShapeDtypeStruct((count, rows, dv), jnp.float32),
+        in_specs=[vmem],
+        out_specs=vmem,
+        scratch_shapes=[
+            pltpu.VMEM((count, 2, rows, dv), jnp.float32),
+            pltpu.VMEM((count, rows, dv), jnp.float32),
+            dma((2,)),
+            dma((count,)),
+            dma((count,)),
+            dma((count,)),
+            dma((count,)),
+        ],
+        compiler_params=pltpu.CompilerParams(collective_id=1, has_side_effects=True),
+        name="suffix_states",
+    )(packed)
+    return out.reshape(local_sum.shape)
 
 
 def block_back(carried, inputs):
@@ -59,17 +268,6 @@
     return (carried, (grad_q, grad_k, grad_v, contrib))
 
 
-def combine(earlier, latter):
-    gain_early, sum_early, term_early, reach_early = earlier
-    gain_late, sum_late, term_late, reach_late = latter
-    return (
-        gain_early * gain_late,
-        gain_late[:, :, None] * sum_early + sum_late,
-        term_early + term_late - jnp.sum(reach_late * sum_early, axis=2),
-        reach_early + gain_early[:, :, None] * reach_late,
-    )
-
-
 def body(
     moe_input,
     out_grad,
@@ -86,8 +284,9 @@
     log_decay,
     block_states,
 ):
-    sp_count = lax.axis_size("sp")
-    experts = sp_count // 2
+    sp_count = sp_size()
+    experts = lax.axis_size("ep")
+    pair = lax.axis_index("pair")
     tok_rows = moe_input.shape[0]
     model_width = moe_input.shape[1]
     capacity = 3 * tok_rows // experts
@@ -113,20 +312,12 @@
     )
     grad_send = jnp.dot(dispatch, scaled, preferred_element_type=jnp.float32).astype(jnp.bfloat16)
 
-    def spread(buffer):
-        doubled = jnp.broadcast_to(
-            buffer.reshape(experts, 1, capacity, send_width), (experts, 2, capacity, send_width)
-        )
-        return doubled.reshape(sp_count * capacity, send_width)
-
-    arrived_tokens, arrived_grads = (
-        lax.all_to_all(spread(token_send), "sp", split_axis=0, concat_axis=0, tiled=True),
-        lax.all_to_all(spread(grad_send), "sp", split_axis=0, concat_axis=0, tiled=True),
-    )
-    arrived_tokens, arrived_grads = (
-        lax.all_gather(arrived_tokens, "tp", axis=1, tiled=True),
-        lax.all_gather(arrived_grads, "tp", axis=1, tiled=True),
-    )
+    arrived_tokens, arrived_grads = dispatch_rows(
+        token_send.reshape(experts, capacity, send_width),
+        grad_send.reshape(experts, capacity, send_width),
+    )
+    arrived_tokens = arrived_tokens.reshape(sp_count * capacity, model_width)
+    arrived_grads = arrived_grads.reshape(sp_count * capacity, model_width)
     gate_mat = gate_w[0]
     up_mat = up_w[0]
     down_mat = down_w[0]
@@ -151,22 +342,25 @@
     partial_value = lax.dot_general(
         d_gate, gate_mat, ACROSS, preferred_element_type=jnp.float32
     ) + lax.dot_general(d_up, up_mat, ACROSS, preferred_element_type=jnp.float32)
-    half_grad = lax.psum_scatter(
-        partial_value.astype(jnp.bfloat16), "tp", scatter_dimension=1, tiled=True
-    )
-    returned = lax.all_to_all(half_grad, "sp", split_axis=0, concat_axis=0, tiled=True)
-    pick_both = jnp.broadcast_to(
-        token_pick.reshape(experts, 1, capacity, tok_rows), (experts, 2, capacity, tok_rows)
-    ).reshape(sp_count * capacity, tok_rows)
-    moe_grad = lax.dot_general(pick_both, returned, DOWNWARD, preferred_element_type=jnp.float32)
+    parts = partial_value.astype(jnp.bfloat16)
+    own_part = lax.dynamic_slice_in_dim(parts, col_start, col_count, 1)
+    other_part = lax.dynamic_slice_in_dim(parts, col_count - col_start, col_count, 1)
+    core_part = lax.ppermute(other_part, "tp", [(0, 1), (1, 0)])
+    half_grad = (own_part.astype(jnp.float32) + core_part.astype(jnp.float32)).astype(jnp.bfloat16)
+    half_grad = half_grad.reshape(2, experts * capacity, col_count)
+    kept = lax.dynamic_index_in_dim(half_grad, pair, 0, False)
+    passed_on = lax.dynamic_index_in_dim(half_grad, 1 - pair, 0, False)
+    pair_part = lax.ppermute(passed_on, "pair", [(0, 1), (1, 0)])
+    both = (kept.astype(jnp.float32) + pair_part.astype(jnp.float32)).astype(jnp.bfloat16)
+    returned = lax.all_to_all(both, "ep", split_axis=0, concat_axis=0, tiled=True)
+    moe_grad = lax.dot_general(token_pick, returned, DOWNWARD, preferred_element_type=jnp.float32)
     grad_mid = (source_grads.astype(jnp.float32) + moe_grad).astype(jnp.bfloat16)
     grad_mid = lax.all_gather(grad_mid, "tp", axis=1, tiled=True)
-    grad_out_weight = lax.psum_scatter(
-        lax.dot_general(grad_mid, mixer_out, DOWNWARD, preferred_element_type=jnp.float32),
-        "sp",
-        scatter_dimension=0,
-        tiled=True,
-    ).T
+    mixer_all = lax.all_gather(mixer_out, SP, axis=0, tiled=True)
+    mid_columns = lax.all_to_all(grad_mid, SP, split_axis=1, concat_axis=0, tiled=True)
+    grad_out_weight = lax.dot_general(
+        mixer_all, mid_columns, DOWNWARD, preferred_element_type=jnp.float32
+    )
     grad_mixed = lax.dot_general(
         grad_mid, out_weight, ACROSS, preferred_element_type=jnp.float32
     ).astype(jnp.bfloat16)
@@ -193,20 +387,11 @@
     fade_out = jnp.exp(device_total[None, None] - position)
     k_fade = k_blocks * fade_out
     reach_sum = jnp.einsum("nshd,nshv->hdv", k_fade, v_blocks, precision=PRECISE)
-    identity = (
-        jnp.ones((heads_local, DK), jnp.float32),
-        jnp.zeros((heads_local, DK, DV), jnp.float32),
-        jnp.zeros((heads_local, DK), jnp.float32),
-        jnp.zeros((heads_local, DK, DV), jnp.float32),
-    )
-    scanned = prefix(
-        (jnp.exp(device_total), local_sum, jnp.sum(contrib, axis=(0, 1)), reach_sum),
-        "sp",
-        combine,
-        identity,
-    )
-    from_right = scanned[1]
-    right_terms = scanned[2]
+    from_right = suffix_states(jnp.exp(device_total), local_sum)
+    own_terms = jnp.sum(contrib, axis=(0, 1)) - jnp.sum(reach_sum * from_right, axis=2)
+    all_terms = lax.all_gather(own_terms.reshape(-1), SP)
+    later = (jnp.arange(sp_count) > sp_index()).astype(jnp.float32)
+    right_terms = jnp.sum(all_terms * later[:, None], axis=0)
     key_part = jnp.einsum("nshv,hdv->nshd", v_blocks, from_right, precision=PRECISE)
     grad_k = grad_k + fade_out * key_part
     grad_v = grad_v + jnp.einsum("nshd,hdv->nshv", k_fade, from_right, precision=PRECISE)
@@ -225,35 +410,37 @@
 
 
 def solution(mesh):
+    sp_count, tp_count = mesh.devices.shape
+    mesh = Mesh(mesh.devices.reshape(sp_count // 2, 2, tp_count), ("ep", "pair", "tp"))
     placed = (
-        P("sp", None),
-        P("sp", None),
-        P("sp", None),
-        P("sp", None),
-        P("sp", None, "tp"),
-        P("sp", None, "tp"),
-        P("sp", "tp", None),
-        P("sp", "tp"),
+        P(SP, None),
+        P(SP, None),
+        P(SP, None),
+        P(SP, None),
+        P(SP, None, "tp"),
+        P(SP, None, "tp"),
+        P(SP, "tp", None),
+        P(SP, "tp"),
         P("tp", None),
-        P("sp", "tp"),
-        P("sp", "tp"),
-        P("sp", "tp"),
-        P("sp", "tp"),
-        P("sp", "tp", None, None),
+        P(SP, "tp"),
+        P(SP, "tp"),
+        P(SP, "tp"),
+        P(SP, "tp"),
+        P(SP, "tp", None, None),
     )
     return jax.shard_map(
         body,
         mesh=mesh,
         in_specs=placed,
         out_specs=(
-            P("sp", "tp"),
-            P("sp", "tp"),
-            P("sp", "tp"),
-            P("sp", "tp"),
-            P("tp", "sp"),
-            P("sp", None, "tp"),
-            P("sp", None, "tp"),
-            P("sp", "tp", None),
+            P(SP, "tp"),
+            P(SP, "tp"),
+            P(SP, "tp"),
+            P(SP, "tp"),
+            P("tp", SP),
+            P(SP, None, "tp"),
+            P(SP, None, "tp"),
+            P(SP, "tp", None),
         ),
         check_vma=False,
     )

time: 390 us -> 297 us (0.76)
  waiting for transfers between devices: 113 us -> 27.1 us
  blocking collectives: 127 us -> 43.2 us
  Pallas kernels: 0 us -> 71.7 us
  local copies, waits for them, and re-layouts: 24.4 us -> 35.4 us
  other arithmetic: 22.7 us -> 15.4 us
    pallas_call x0 -> x2, Pallas kernels: none -> 71.7 us  [the longest x1 53.2 us: dispatch_rows(): pl.pallas_call(functools.partial(dispatch_kernel, experts, width), out_sh...]
    reduce_scatter x2 -> x0, waiting for transfers between devices: 50.6 us -> none  [the longest x1 41.1 us: body(): lax.psum_scatter(lax.dot_general(grad_mid, mixer_out, DOWNWARD, preferred...]
    all_to_all x1 -> x0, blocking collectives: 44.5 us -> none  [body(): lax.all_to_all(spread(grad_send), 'sp', split_axis=0, concat_axis=0, tile...]
    all_to_all x2, waiting for transfers between devices: 62.1 us -> 18.3 us  [the longest x1 18.3 us: body(): lax.all_to_all(both, 'ep', split_axis=0, concat_axis=0, tiled=True)]
    all_gather x2 -> x1, blocking collectives: 80.4 us -> 41 us  [body(): all_terms = lax.all_gather(own_terms.reshape(-1), SP)]
    reduce_sum x16 -> x2, other arithmetic: 17.2 us -> 0.19 us  [the longest x1 0.11 us: body(): jnp.sum(contrib, axis=(0, 1)) - jnp.sum(reach_sum * from_right, axis=2)]
    ppermute x0 -> x2, waiting for transfers between devices: none -> 8.78 us  [the longest x1 7.36 us: body(): pair_part = lax.ppermute(passed_on, 'pair', [(0, 1), (1, 0)])]
    convert_element_type x0 -> x3, other arithmetic: none -> 4.87 us  [the longest x1 2.54 us: body(): (own_part.astype(jnp.float32) + core_part.astype(jnp.float32)).astype(jnp...]
  transfers between devices with their start and end apart: 8 -> 5, of which waited for: 4 -> 3; matrix products, arithmetic and copies ran while one was open for 23% -> 24% of each run, Pallas kernels for 0% -> 6%
where the time goes in v1:
time: 297 us; the launch traced here: 296 us
  matrix products  71.7 us (24%)
  Pallas kernels  71.7 us (24%)
  blocking collectives  43.2 us (15%)
  local copies, waits for them, and re-layouts  35.4 us (12%)
  waiting for transfers between devices  27.1 us (9%)
  starting transfers between devices  16.3 us (5%)
  other arithmetic  15.4 us (5%)
  between operations  14.5 us (5%)
    pallas_call x1, Pallas kernels, dispatch_rows(): pl.pallas_call(functools.partial(dispatch_kernel, experts, width), out_sh...  53.2 us
    all_gather x1, blocking collectives, body(): all_terms = lax.all_gather(own_terms.reshape(-1), SP)  41 us
    pallas_call x1, Pallas kernels, suffix_states(): pl.pallas_call(functools.partial(suffix_kernel, count, rows), out_shape=j...  18.5 us
    all_to_all x1, waiting for transfers between devices, body(): lax.all_to_all(both, 'ep', split_axis=0, concat_axis=0, tiled=True)  18.3 us
    all_to_all x1, starting transfers between devices, body(): lax.all_to_all(both, 'ep', split_axis=0, concat_axis=0, tiled=True)  12 us
    dot_general x1, matrix products, body(): lax.dot_general(d_up, up_mat, ACROSS, preferred_element_type=jnp.float32)  9.42 us
    dot_general x1, matrix products, body(): lax.dot_general(arrived_tokens, d_up, DOWNWARD, preferred_element_type=jn...  7.75 us
    dot_general x1, matrix products, body(): lax.dot_general(arrived_tokens, d_gate, DOWNWARD, preferred_element_type=...  7.75 us
  transfers between devices with their start and end apart: 5, of which 3 were waited for; matrix products, arithmetic and copies ran while one was open for 24% of the time, Pallas kernels for 6%

profile of v1, /device:TPU:0, one launch (start us, length us, event | category | flops | bytes accessed | tf_op | source)
XLA Modules:
  0.0 295.5 jit_solution(518941400195643938)
XLA Ops:
  14.9 2.2 convolution_convert_fusion.1
  18.4 53.2 %dispatch_rows.1 = (bf16[2,8,48,2048]{3,2,1,0:T(8,128)(2,1)}, bf16[2,8,48,2048]{3,2,1,0:T(8,128)(2,1)}) custom-call(bf16[8,48,1024]{2,1,0:T(8,128)(2,1)} %bitcast.247, bf16[8,48,1024]{2,1,0:T(8,128)(2,1)} %bitcast.248), custom_call_target="tpu_custom_call" | custom-call | tf_op jit(solution)/shard_map/dispatch_rows/pallas_call | solution.py:131
  71.7 6.5 %fusion.30 = f32[768,896]{1,0:T(8,128)S(1)} fusion(bf16[768,2048]{1,0:T(8,128)(2,1)} %bitcast.259, bf16[1,2048,896]{2,1,0:T(8,128)(2,1)} %param.20), kind=kOutput, calls=%fused_computation.57 | convolution fusion | flops 2818572288 | bytes 9568256 | tf_op jit(solution)/shard_map/dot_general | solution.py:324
  78.3 3.4 %fusion.34 = f32[768,896]{1,0:T(8,128)S(1)} fusion(bf16[768,2048]{1,0:T(8,128)(2,1)S(1)} %bitcast.262, bf16[1,2048,896]{2,1,0:T(8,128)(2,1)S(1)} %copy-done.15), kind=kOutput, calls=%fused_computation.61 | convolution fusion | flops 2818572288 | bytes 9568256 | tf_op jit(solution)/shard_map/dot_general | solution.py:325
  82.2 5.1 %multiply_convert_fusion.1 = (bf16[768,896]{1,0:T(8,128)(2,1)}, bf16[768,896]{1,0:T(8,128)(2,1)S(1)}) fusion(f32[768,896]{1,0:T(8,128)S(1)} %fusion.30, f32[768,896]{1,0:T(8,128)S(1)} %fusion.34, bf16[768,2048]{1,0:T(8,128)(2,1)S(1)} %bitcast.257, bf16[1,896,2048]{2,1,0:T(8,128)(2,1)S(1)} %copy-done.13), kind=kOutput, calls=%fused_computation.70 | convolution fusion | flops 2827517952 | bytes 15073280 | tf_op jit(solution)/shard_map/dot_general | solution.py:328
  88.5 5.4 %fusion.28 = f32[768,2048]{1,0:T(8,128)} fusion(bf16[768,896]{1,0:T(8,128)(2,1)S(1)} %get-tuple-element.430, bf16[1,2048,896]{2,1,0:T(8,128)(2,1)S(1)} %copy-done.14), kind=kOutput, calls=%fused_computation.55 | convolution fusion | flops 2818572288 | bytes 11337728 | tf_op jit(solution)/shard_map/dot_general | solution.py:342
  93.9 9.4 %add_convert_fusion = bf16[768,2048]{1,0:T(8,128)(2,1)} fusion(f32[768,2048]{1,0:T(8,128)} %fusion.28, bf16[768,896]{1,0:T(8,128)(2,1)} %get-tuple-element.429, bf16[1,2048,896]{2,1,0:T(8,128)(2,1)} %param.21), kind=kOutput, calls=%fused_computation.54 | convolution fusion | flops 2821718016 | bytes 14483456 | tf_op jit(solution)/shard_map/dot_general | solution.py:344
  103.3 2.7 constant_dynamic-slice_fusion.4
  109.8 2.5 add_convert_fusion.1
  120.4 7.8 %convert_bitcast_fusion.1 = bf16[1,2048,896]{2,1,0:T(8,128)(2,1)} fusion(bf16[768,2048]{1,0:T(8,128)(2,1)} %bitcast.260, bf16[768,896]{1,0:T(8,128)(2,1)} %get-tuple-element.429), kind=kOutput, calls=%fused_computation.66 | convolution fusion | flops 2820407296 | bytes 8192000 | tf_op jit(solution)/shard_map/dot_general | solution.py:339
  128.2 7.4 %collective-permute-done.1 = bf16[384,1024]{1,0:T(8,128)(2,1)} collective-permute-done((bf16[384,1024]{1,0:T(8,128)(2,1)}, bf16[384,1024]{1,0:T(8,128)(2,1)}, u32[]{:S(2)}, u32[]{:S(2)}) %collective-permute-start.1) | collective-permute-done | bytes 786464 | tf_op jit(solution)/shard_map/ppermute | solution.py:353
  135.6 2.3 fusion.40
  137.9 12.0 %all-to-all-start = ((bf16[8,48,1024]{2,1,0:T(8,128)(2,1)}), bf16[8,48,1024]{2,1,0:T(8,128)(2,1)S(1)}, u32[]{:S(2)}, u32[]{:S(2)}) async-start(bf16[8,48,1024]{2,1,0:T(8,128)(2,1)} %bitcast.12), calls=%async_computation | async-start | bytes 1572864 | tf_op jit(solution)/shard_map/all_to_all | solution.py:355
  149.9 7.8 %convert_bitcast_fusion.2 = bf16[1,2048,896]{2,1,0:T(8,128)(2,1)} fusion(bf16[768,2048]{1,0:T(8,128)(2,1)} %bitcast.261, bf16[768,896]{1,0:T(8,128)(2,1)} %copy-done.19), kind=kOutput, calls=%fused_computation.67 | convolution fusion | flops 2820407296 | bytes 8192000 | tf_op jit(solution)/shard_map/dot_general | solution.py:336
  157.7 4.7 %convert_bitcast_fusion = bf16[1,896,2048]{2,1,0:T(8,128)(2,1)} fusion(bf16[768,2048]{1,0:T(8,128)(2,1)S(1)} %bitcast.258, f32[768,896]{1,0:T(8,128)S(1)} %copy-done.23, f32[768,896]{1,0:T(8,128)S(1)} %copy-done.21), kind=kOutput, calls=%fused_computation.65 | convolution fusion | flops 2824536064 | bytes 12320768 | tf_op jit(solution)/shard_map/dot_general | solution.py:333
  162.3 18.3 %all-to-all-done = bf16[8,48,1024]{2,1,0:T(8,128)(2,1)S(1)} async-done(((bf16[8,48,1024]{2,1,0:T(8,128)(2,1)}), bf16[8,48,1024]{2,1,0:T(8,128)(2,1)S(1)}, u32[]{:S(2)}, u32[]{:S(2)}) %all-to-all-start) | async-done | bytes 786464 | tf_op jit(solution)/shard_map/all_to_all | solution.py:355
  181.9 2.2 all_gather.9
  188.7 19.0 %while.23 = (s32[]{:T(128)}, f32[4,64,128]{2,1,0:T(8,128)S(1)}, bf16[2,64,4,64]{1,3,2,0:T(8,128)(2,1)}, f32[2,64,4,64]{1,3,0,2:T(8,128)}, f32[2,64,4,128]{3,1,0,...) while((s32[]{:T(128)}, f32[4,64,128]{2,1,0:T(8,128)S(1)}, ...), condition=%wide.region_6.7_spmd.clone, body=%wide.region_4.6_spmd.clone.sunk | while | flops 190324736 | bytes 5430457 | solution.py:379
  208.5 18.5 %suffix_states.1 = f32[16,16,128]{2,1,0:T(8,128)} custom-call(f32[16,2,16,128]{3,2,1,0:T(8,128)} %pad_maximum_fusion.state), custom_call_target="tpu_custom_call" | custom-call | tf_op jit(solution)/shard_map/suffix_states/pallas_call | solution.py:221
  227.0 2.0 copy_bitcast_fusion.8
  229.1 3.8 %all-to-all-start.1 = ((bf16[128,16,128]{2,0,1:T(8,128)(2,1)}), bf16[128,16,128]{2,0,1:T(8,128)(2,1)S(1)}, u32[]{:S(2)}, u32[]{:S(2)}) async-start(bf16[128,16,128]{2,0,1:T(8,128)(2,1)} %copy_bitcast_fusion.8), calls=%async_computation.1 | async-start | bytes 1048576 | tf_op jit(solution)/shard_map/all_to_all | solution.py:360
  232.8 2.4 copy_subtract_fusion
  243.1 41.0 %all-gather = f32[16,1,256]{2,1,0:T(1,128)S(1)} all-gather(f32[1,1,256]{2,1,0:T(1,128)S(1)} %reshape.209), channel_id=1, replica_groups=mesh['ep'=8,'pair'=2,'tp'=2] {'ep','pair'}, dimensions={0}, use_global_device_ids=true | all-gather | bytes 17408 | tf_op jit(solution)/shard_map/all_gather | solution.py:392
  285.8 2.1 convolution_bitcast_fusion.4
  (159 shorter events, 58.2 us)
Async XLA Ops:
  7.2 177.7 %copy-start = (bf16[512,2048]{1,0:T(8,128)(2,1)S(1)}, bf16[512,2048]{1,0:T(8,128)(2,1)}, u32[]{:S(2)}) copy-start(bf16[512,2048]{1,0:T(8,128)(2,1)} %param.24) | copy-start | bytes 6291460
  7.2 7.5 %copy-start.12 = (f32[128,2]{0,1:T(2,128)S(1)}, f32[128,2]{0,1:T(2,128)}, u32[]{:S(2)}) copy-start(f32[128,2]{0,1:T(2,128)} %param.19) | copy-start | bytes 3076
  7.2 278.6 %all-gather.3.cloned.1.call-start = ((), (), s32[]{:S(2)}) async-start(), calls=%async_computation.2 | async-start | bytes 2228224 | tf_op jit(solution)/shard_map/all_gather | solution.py:359
  71.7 6.6 %copy-start.15 = (bf16[1,2048,896]{2,1,0:T(8,128)(2,1)S(1)}, bf16[1,2048,896]{2,1,0:T(8,128)(2,1)}, u32[]{:S(2)}) copy-start(bf16[1,2048,896]{2,1,0:T(8,128)(2,1)} %param.21) | copy-start | bytes 11010052
  71.7 6.6 %copy-start.18 = (bf16[2,8,48,2048]{3,2,1,0:T(8,128)(2,1)S(1)}, bf16[2,8,48,2048]{3,2,1,0:T(8,128)(2,1)}, u32[]{:S(2)}) copy-start(bf16[2,8,48,2048]{3,2,1,0:T(8,128)(2,1)} %get-tuple-element.251) | copy-start | bytes 9437188
  78.2 3.5 %copy-start.20 = (f32[768,896]{1,0:T(8,128)}, f32[768,896]{1,0:T(8,128)S(1)}, u32[]{:S(2)}) copy-start(f32[768,896]{1,0:T(8,128)S(1)} %fusion.30) | copy-start | bytes 8257540
  78.3 4.0 %copy-start.16 = (bf16[2,8,48,2048]{3,2,1,0:T(8,128)(2,1)S(1)}, bf16[2,8,48,2048]{3,2,1,0:T(8,128)(2,1)}, u32[]{:S(2)}) copy-start(bf16[2,8,48,2048]{3,2,1,0:T(8,128)(2,1)} %get-tuple-element.250) | copy-start | bytes 9437188
  81.7 5.7 %copy-start.22 = (f32[768,896]{1,0:T(8,128)}, f32[768,896]{1,0:T(8,128)S(1)}, u32[]{:S(2)}) copy-start(f32[768,896]{1,0:T(8,128)S(1)} %fusion.34) | copy-start | bytes 8257540
  82.2 6.3 %copy-start.14 = (bf16[1,2048,896]{2,1,0:T(8,128)(2,1)S(1)}, bf16[1,2048,896]{2,1,0:T(8,128)(2,1)}, u32[]{:S(2)}) copy-start(bf16[1,2048,896]{2,1,0:T(8,128)(2,1)} %param.20) | copy-start | bytes 11010052
  106.0 3.8 %collective-permute-start = (bf16[768,1024]{1,0:T(8,128)(2,1)}, bf16[768,1024]{1,0:T(8,128)(2,1)}, u32[]{:S(2)}, u32[]{:S(2)}) collective-permute-start(bf16[768,1024]{1,0:T(8,128)(2,1)} %constant_dynamic-slice_fusion.4), channel_id=1, source_target_pairs={{0,1},{1,0},{2,3},{3,2},{4,5},{5,4},{6,7},{7,6},{8,9},{9,8},{10,11... | collective-permute-start | bytes 4718600 | tf_op jit(solution)/shard_map/ppermute | solution.py:348
  108.4 6.9 %copy-start.9 = (bf16[128,512]{1,0:T(8,128)(2,1)S(1)}, bf16[128,512]{1,0:T(8,128)(2,1)}, u32[]{:S(2)}) copy-start(bf16[128,512]{1,0:T(8,128)(2,1)} %param.27) | copy-start | bytes 393220
  108.4 7.7 %copy-start.10 = (bf16[128,256]{1,0:T(8,128)(2,1)S(1)}, bf16[128,256]{1,0:T(8,128)(2,1)}, u32[]{:S(2)}) copy-start(bf16[128,256]{1,0:T(8,128)(2,1)} %param.26) | copy-start | bytes 196612
  108.4 8.6 %copy-start.11 = (bf16[128,256]{1,0:T(8,128)(2,1)S(1)}, bf16[128,256]{1,0:T(8,128)(2,1)}, u32[]{:S(2)}) copy-start(bf16[128,256]{1,0:T(8,128)(2,1)} %param.25) | copy-start | bytes 196612
  114.5 21.1 %collective-permute-start.1 = (bf16[384,1024]{1,0:T(8,128)(2,1)}, bf16[384,1024]{1,0:T(8,128)(2,1)}, u32[]{:S(2)}, u32[]{:S(2)}) collective-permute-start(bf16[384,1024]{1,0:T(8,128)(2,1)} %dynamic-slice_bitcast_fusion), channel_id=1, source_target_pairs={{0,2},{2,0},{1,3},{3,1},{4,6},{6,4},{5,7},{7,5},{8,10},{10,8},{9,1... | collective-permute-start | bytes 2359304 | tf_op jit(solution)/shard_map/ppermute | solution.py:353
  115.4 12.8 %copy-start.6 = (bf16[2,64,4,128]{3,2,1,0:T(4,128)(2,1)}, bf16[2,64,4,128]{3,2,1,0:T(4,128)(2,1)S(1)}, u32[]{:S(2)}) copy-start(bf16[2,64,4,128]{3,2,1,0:T(4,128)(2,1)S(1)} %reshape.198) | copy-start | bytes 393220
  120.4 15.1 %copy-start.2 = (bf16[768,1024]{1,0:T(8,128)(2,1)S(1)}, bf16[768,1024]{1,0:T(8,128)(2,1)}, u32[]{:S(2)}) copy-start(bf16[768,1024]{1,0:T(8,128)(2,1)} %copy-done.1) | copy-start | bytes 4718596
  137.9 42.7 %all-to-all-start = ((bf16[8,48,1024]{2,1,0:T(8,128)(2,1)}), bf16[8,48,1024]{2,1,0:T(8,128)(2,1)S(1)}, u32[]{:S(2)}, u32[]{:S(2)}) async-start(bf16[8,48,1024]{2,1,0:T(8,128)(2,1)} %bitcast.12), calls=%async_computation | async-start | bytes 1572864 | tf_op jit(solution)/shard_map/all_to_all | solution.py:355
  149.9 7.8 %copy-start.17 = (bf16[2,8,48,2048]{3,2,1,0:T(8,128)(2,1)S(1)}, bf16[2,8,48,2048]{3,2,1,0:T(8,128)(2,1)}, u32[]{:S(2)}) copy-start(bf16[2,8,48,2048]{3,2,1,0:T(8,128)(2,1)} %get-tuple-element.250) | copy-start | bytes 9437188
  149.9 7.8 %copy-start.21 = (f32[768,896]{1,0:T(8,128)S(1)}, f32[768,896]{1,0:T(8,128)}, u32[]{:S(2)}) copy-start(f32[768,896]{1,0:T(8,128)} %copy-done.20) | copy-start | bytes 8257540
  149.9 7.8 %copy-start.23 = (f32[768,896]{1,0:T(8,128)S(1)}, f32[768,896]{1,0:T(8,128)}, u32[]{:S(2)}) copy-start(f32[768,896]{1,0:T(8,128)} %copy-done.22) | copy-start | bytes 8257540
  207.6 25.2 %copy-start.4 = (f32[2,64,4,64]{1,3,2,0:T(8,128)S(1)}, f32[2,64,4,64]{1,3,2,0:T(8,128)}, u32[]{:S(2)}) copy-start(f32[2,64,4,64]{1,3,2,0:T(8,128)} %get-tuple-element.256) | copy-start | bytes 393220
  207.6 25.2 %copy-start.7 = (bf16[2,64,4,128]{3,2,1,0:T(4,128)(2,1)S(1)}, bf16[2,64,4,128]{3,2,1,0:T(4,128)(2,1)}, u32[]{:S(2)}) copy-start(bf16[2,64,4,128]{3,2,1,0:T(4,128)(2,1)} %copy-done.6) | copy-start | bytes 393220
  227.0 8.5 %copy-start.5 = (f32[16,16,128]{2,1,0:T(8,128)S(1)}, f32[16,16,128]{2,1,0:T(8,128)}, u32[]{:S(2)}) copy-start(f32[16,16,128]{2,1,0:T(8,128)} %suffix_states.1) | copy-start | bytes 393220
  229.1 56.7 %all-to-all-start.1 = ((bf16[128,16,128]{2,0,1:T(8,128)(2,1)}), bf16[128,16,128]{2,0,1:T(8,128)(2,1)S(1)}, u32[]{:S(2)}, u32[]{:S(2)}) async-start(bf16[128,16,128]{2,0,1:T(8,128)(2,1)} %copy_bitcast_fusion.8), calls=%async_computation.1 | async-start | bytes 1048576 | tf_op jit(solution)/shard_map/all_to_all | solution.py:360
  (5 other events, 9.7 us)
Sparse Core Ops, SparseCore 0:
  106.6 74.2 all-gather.2

commit v2 on v1

--- a/solution.py
+++ b/solution.py
@@ -147,7 +147,10 @@
     )(token_send, grad_send)
 
 
-def suffix_kernel(count, rows, state, out, held, result, local_sem, go_send, go_recv, back_send, back_recv):
+def suffix_kernel(
+    count, rows, state, reach, terms, out, right, held, result, gathered,
+    local_sem, go_send, go_recv, back_send, back_recv, term_send, term_recv,
+):
     me = sp_index()
     t = lax.axis_index("tp")
 
@@ -200,12 +203,37 @@
     back(0).wait()
     for k in range(1, count):
         landed(out, back_send, back_recv, k)
+    lanes = lax.broadcasted_iota(jnp.int32, (rows, state.shape[-1]), 1)
+    places = lax.broadcasted_iota(jnp.int32, (rows, state.shape[-1]), 0)
+    groups = [jnp.zeros((1, 128), jnp.float32) for _ in range(terms.shape[0])]
+    for c in range(count):
+        dots = jnp.sum(reach[c] * out[c], axis=1, keepdims=True)
+        picked = jnp.where(lanes == places + (c * rows) % 128, dots, 0.0)
+        groups[c * rows // 128] += jnp.sum(picked, axis=0, keepdims=True)
+    gathered[me] = terms[...] - jnp.concatenate(groups, axis=0)
+
+    def tell(k):
+        return pltpu.make_async_remote_copy(
+            src_ref=gathered.at[me], dst_ref=gathered.at[me], send_sem=term_send.at[k],
+            recv_sem=term_recv.at[k], device_id=place(lax.rem(me + k, count)), device_id_type=MESH,
+        )
+
     for k in range(1, count):
         go(k).wait_send()
         back(k).wait_send()
-
-
-def suffix_states(gain, local_sum):
+    for k in range(1, count):
+        tell(k).start()
+    for k in range(1, count):
+        landed(gathered, term_send, term_recv, k)
+    summed = jnp.zeros(terms.shape, jnp.float32)
+    for i in range(count):
+        summed += jnp.where(i > me, gathered[i], 0.0)
+    right[...] = summed
+    for k in range(1, count):
+        tell(k).wait_send()
+
+
+def suffix_states(gain, local_sum, reach_sum, terms):
     count = sp_size()
     heads, dk, dv = local_sum.shape
     rows = heads * dk // count
@@ -218,15 +246,22 @@
     )
     vmem = pl.BlockSpec(memory_space=pltpu.VMEM)
     dma = pltpu.SemaphoreType.DMA
-    out = pl.pallas_call(
+    terms = terms.reshape(heads * dk // 128, 128)
+    out, right = pl.pallas_call(
         functools.partial(suffix_kernel, count, rows),
-        out_shape=jax.ShapeDtypeStruct((count, rows, dv), jnp.float32),
-        in_specs=[vmem],
-        out_specs=vmem,
+        out_shape=(
+            jax.ShapeDtypeStruct((count, rows, dv), jnp.float32),
+            jax.ShapeDtypeStruct(terms.shape, jnp.float32),
+        ),
+        in_specs=[vmem] * 3,
+        out_specs=(vmem, vmem),
         scratch_shapes=[
             pltpu.VMEM((count, 2, rows, dv), jnp.float32),
             pltpu.VMEM((count, rows, dv), jnp.float32),
+            pltpu.VMEM((count,) + terms.shape, jnp.float32),
             dma((2,)),
+            dma((count,)),
+            dma((count,)),
             dma((count,)),
             dma((count,)),
             dma((count,)),
@@ -234,8 +269,166 @@
         ],
         compiler_params=pltpu.CompilerParams(collective_id=1, has_side_effects=True),
         name="suffix_states",
-    )(packed)
-    return out.reshape(local_sum.shape)
+    )(packed, reach_sum.reshape(count, rows, dv), terms)
+    return out.reshape(local_sum.shape), right.reshape(1, -1)
+
+
+def return_kernel(
+    experts, width, steps, parts, tokens, grads, hidden, d_gate, d_up,
+    returned, gate_out, up_out, down_out,
+    core_held, pair_stage, pair_held, send_stage, gate_stage, up_stage, down_stage,
+    out_sem, local_sem, core_send, core_recv, pair_send, pair_recv, back_send, back_recv,
+):
+    e, p, t = lax.axis_index("ep"), lax.axis_index("pair"), lax.axis_index("tp")
+    barrier = pltpu.get_barrier_semaphore()
+    for k in range(1, experts):
+        pl.semaphore_signal(
+            barrier, inc=1, device_id=(lax.rem(e + k, experts), p, t), device_id_type=MESH
+        )
+    pl.semaphore_signal(barrier, inc=1, device_id=(e, 1 - p, t), device_id_type=MESH)
+    pl.semaphore_signal(barrier, inc=1, device_id=(e, p, 1 - t), device_id_type=MESH)
+    pl.semaphore_wait(barrier, experts + 1)
+    own_columns = pl.ds(pl.multiple_of(t * width, 128), width)
+    core_columns = pl.ds(pl.multiple_of((1 - t) * width, 128), width)
+
+    def owner(k):
+        return lax.rem(e + 1 + k, experts)
+
+    def core_copy(which, k):
+        side = 1 - p if which == 0 else p
+        return pltpu.make_async_remote_copy(
+            src_ref=parts.at[side, owner(k), :, core_columns],
+            dst_ref=core_held.at[which, k],
+            send_sem=core_send.at[which, k],
+            recv_sem=core_recv.at[which, k],
+            device_id=(e, p, 1 - t),
+            device_id_type=MESH,
+        )
+
+    def pair_copy(k):
+        return pltpu.make_async_remote_copy(
+            src_ref=pair_stage.at[k], dst_ref=pair_held.at[k], send_sem=pair_send.at[k],
+            recv_sem=pair_recv.at[k], device_id=(e, 1 - p, t), device_id_type=MESH,
+        )
+
+    def back_copy(k):
+        return pltpu.make_async_remote_copy(
+            src_ref=send_stage.at[k], dst_ref=returned.at[e], send_sem=back_send.at[k],
+            recv_sem=back_recv.at[k], device_id=(owner(k), p, t), device_id_type=MESH,
+        )
+
+    def half_of(which, k):
+        side = 1 - p if which == 0 else p
+        mine = parts[side, owner(k), :, own_columns].astype(jnp.float32)
+        return (mine + core_held[which, k].astype(jnp.float32)).astype(jnp.bfloat16)
+
+    for which in range(2):
+        for k in range(experts):
+            core_copy(which, k).start()
+    for k in range(experts):
+        core_copy(0, k).wait_recv()
+        pair_stage[k] = half_of(0, k)
+        if k:
+            pair_copy(k - 1).start()
+    pair_copy(experts - 1).start()
+    for k in range(experts):
+        core_copy(1, k).wait_recv()
+
+    def down_step(i, carry):
+        cut = pl.ds(pl.multiple_of(i * 128, 128), 128)
+        down_stage[cut, :] = lax.dot_general(
+            hidden[:, cut], grads[...], DOWNWARD, preferred_element_type=jnp.float32
+        ).astype(jnp.bfloat16)
+        pltpu.make_async_copy(down_stage.at[cut], down_out.at[cut], out_sem.at[0]).start()
+        return carry
+
+    lax.fori_loop(0, hidden.shape[1] // 128, down_step, 0)
+    span = tokens.shape[1] // steps
+    each = experts // steps
+
+    def weight_step(i, carry):
+        cut = pl.ds(pl.multiple_of(i * span, span), span)
+        gate_stage[cut, :] = lax.dot_general(
+            tokens[:, cut], d_gate[...], DOWNWARD, preferred_element_type=jnp.float32
+        ).astype(jnp.bfloat16)
+        for j in range(each):
+            k = i * each + j
+            pair_copy(k).wait_recv()
+            total = half_of(1, k).astype(jnp.float32) + pair_held[k].astype(jnp.float32)
+            send_stage[k] = total.astype(jnp.bfloat16)
+        up_stage[cut, :] = lax.dot_general(
+            tokens[:, cut], d_up[...], DOWNWARD, preferred_element_type=jnp.float32
+        ).astype(jnp.bfloat16)
+        for j in range(each):
+            k = i * each + j
+
+            @pl.when(k < experts - 1)
+            def _():
+                back_copy(k).start()
+
+        pltpu.make_async_copy(gate_stage.at[cut], gate_out.at[cut], out_sem.at[1]).start()
+        pltpu.make_async_copy(up_stage.at[cut], up_out.at[cut], out_sem.at[2]).start()
+        return carry
+
+    lax.fori_loop(0, steps, weight_step, 0)
+    own = pltpu.make_async_copy(send_stage.at[experts - 1], returned.at[e], local_sem)
+    own.start()
+    own.wait()
+    for k in range(experts - 1):
+        source = lax.rem(e - 1 - k + experts, experts)
+        pltpu.make_async_remote_copy(
+            src_ref=returned.at[source], dst_ref=returned.at[source], send_sem=back_send.at[k],
+            recv_sem=back_recv.at[k], device_id=(source, p, t), device_id_type=MESH,
+        ).wait_recv()
+    for k in range(experts):
+        core_copy(0, k).wait_send()
+        core_copy(1, k).wait_send()
+        pair_copy(k).wait_send()
+        if k < experts - 1:
+            back_copy(k).wait_send()
+    pltpu.make_async_copy(down_stage, down_out, out_sem.at[0]).wait()
+    pltpu.make_async_copy(gate_stage, gate_out, out_sem.at[1]).wait()
+    pltpu.make_async_copy(up_stage, up_out, out_sem.at[2]).wait()
+
+
+def return_rows(parts, tokens, grads, hidden, d_gate, d_up):
+    _, experts, capacity, model_width = parts.shape
+    width = model_width // 2
+    units = hidden.shape[1]
+    half = (experts, capacity, width)
+    vmem = pl.BlockSpec(memory_space=pltpu.VMEM)
+    hbm = pl.BlockSpec(memory_space=pl.ANY)
+    dma = pltpu.SemaphoreType.DMA
+    wide, tall = (model_width, units), (units, model_width)
+    kind = jnp.bfloat16
+    shape = jax.ShapeDtypeStruct
+    return pl.pallas_call(
+        functools.partial(return_kernel, experts, width, min(8, experts)),
+        out_shape=(shape(half, kind), shape(wide, kind), shape(wide, kind), shape(tall, kind)),
+        in_specs=[vmem] * 6,
+        out_specs=(vmem, hbm, hbm, hbm),
+        scratch_shapes=[
+            pltpu.VMEM((2,) + half, kind),
+            pltpu.VMEM(half, kind),
+            pltpu.VMEM(half, kind),
+            pltpu.VMEM(half, kind),
+            pltpu.VMEM(wide, kind),
+            pltpu.VMEM(wide, kind),
+            pltpu.VMEM(tall, kind),
+            dma((3,)),
+            dma,
+            dma((2, experts)),
+            dma((2, experts)),
+            dma((experts,)),
+            dma((experts,)),
+            dma((experts,)),
+            dma((experts,)),
+        ],
+        compiler_params=pltpu.CompilerParams(
+            collective_id=2, has_side_effects=True, vmem_limit_bytes=60 * 1024 * 1024
+        ),
+        name="return_rows",
+    )(parts, tokens, grads, hidden, d_gate, d_up)
 
 
 def block_back(carried, inputs):
@@ -286,7 +479,6 @@
 ):
     sp_count = sp_size()
     experts = lax.axis_size("ep")
-    pair = lax.axis_index("pair")
     tok_rows = moe_input.shape[0]
     model_width = moe_input.shape[1]
     capacity = 3 * tok_rows // experts
@@ -330,29 +522,19 @@
     d_gate = (d_hidden * up_pre * sigmoid_gate * (1.0 + gate_pre * (1.0 - sigmoid_gate))).astype(
         jnp.bfloat16
     )
-    grad_down = lax.dot_general(
-        hidden, arrived_grads, DOWNWARD, preferred_element_type=jnp.float32
-    ).astype(jnp.bfloat16)
-    grad_gate = lax.dot_general(
-        arrived_tokens, d_gate, DOWNWARD, preferred_element_type=jnp.float32
-    ).astype(jnp.bfloat16)
-    grad_up = lax.dot_general(
-        arrived_tokens, d_up, DOWNWARD, preferred_element_type=jnp.float32
-    ).astype(jnp.bfloat16)
     partial_value = lax.dot_general(
         d_gate, gate_mat, ACROSS, preferred_element_type=jnp.float32
     ) + lax.dot_general(d_up, up_mat, ACROSS, preferred_element_type=jnp.float32)
     parts = partial_value.astype(jnp.bfloat16)
-    own_part = lax.dynamic_slice_in_dim(parts, col_start, col_count, 1)
-    other_part = lax.dynamic_slice_in_dim(parts, col_count - col_start, col_count, 1)
-    core_part = lax.ppermute(other_part, "tp", [(0, 1), (1, 0)])
-    half_grad = (own_part.astype(jnp.float32) + core_part.astype(jnp.float32)).astype(jnp.bfloat16)
-    half_grad = half_grad.reshape(2, experts * capacity, col_count)
-    kept = lax.dynamic_index_in_dim(half_grad, pair, 0, False)
-    passed_on = lax.dynamic_index_in_dim(half_grad, 1 - pair, 0, False)
-    pair_part = lax.ppermute(passed_on, "pair", [(0, 1), (1, 0)])
-    both = (kept.astype(jnp.float32) + pair_part.astype(jnp.float32)).astype(jnp.bfloat16)
-    returned = lax.all_to_all(both, "ep", split_axis=0, concat_axis=0, tiled=True)
+    returned, grad_gate, grad_up, grad_down = return_rows(
+        parts.reshape(2, experts, capacity, model_width),
+        arrived_tokens,
+        arrived_grads,
+        hidden,
+        d_gate,
+        d_up,
+    )
+    returned = returned.reshape(experts * capacity, col_count)
     moe_grad = lax.dot_general(token_pick, returned, DOWNWARD, preferred_element_type=jnp.float32)
     grad_mid = (source_grads.astype(jnp.float32) + moe_grad).astype(jnp.bfloat16)
     grad_mid = lax.all_gather(grad_mid, "tp", axis=1, tiled=True)
@@ -387,16 +569,14 @@
     fade_out = jnp.exp(device_total[None, None] - position)
     k_fade = k_blocks * fade_out
     reach_sum = jnp.einsum("nshd,nshv->hdv", k_fade, v_blocks, precision=PRECISE)
-    from_right = suffix_states(jnp.exp(device_total), local_sum)
-    own_terms = jnp.sum(contrib, axis=(0, 1)) - jnp.sum(reach_sum * from_right, axis=2)
-    all_terms = lax.all_gather(own_terms.reshape(-1), SP)
-    later = (jnp.arange(sp_count) > sp_index()).astype(jnp.float32)
-    right_terms = jnp.sum(all_terms * later[:, None], axis=0)
+    from_right, right_terms = suffix_states(
+        jnp.exp(device_total), local_sum, reach_sum, jnp.sum(contrib, axis=(0, 1))
+    )
     key_part = jnp.einsum("nshv,hdv->nshd", v_blocks, from_right, precision=PRECISE)
     grad_k = grad_k + fade_out * key_part
     grad_v = grad_v + jnp.einsum("nshd,hdv->nshv", k_fade, from_right, precision=PRECISE)
     contrib = (contrib - k_fade * key_part).reshape(tok_rows, heads_local * DK)
-    grad_decay = jnp.flip(jnp.cumsum(jnp.flip(contrib, 0), axis=0), 0) + right_terms.reshape(1, -1)
+    grad_decay = jnp.flip(jnp.cumsum(jnp.flip(contrib, 0), axis=0), 0) + right_terms
     return (
         grad_q.reshape(tok_rows, heads_local * DK).astype(jnp.bfloat16),
         grad_k.reshape(tok_rows, heads_local * DK).astype(jnp.bfloat16),

time: 297 us -> 243 us (0.82)
  Pallas kernels: 71.7 us -> 122 us
  blocking collectives: 43.2 us -> 2.18 us
  waiting for transfers between devices: 27.1 us -> 0.69 us
  matrix products: 71.7 us -> 48.2 us
  starting transfers between devices: 16.3 us -> 10 us
  other arithmetic: 15.4 us -> 9.75 us
    pallas_call x1 -> x2, Pallas kernels: 18.5 us -> 69.2 us  [the longest x1 39.8 us: return_rows(): pl.pallas_call(functools.partial(return_kernel, experts, width, min(8, ex...]
    all_gather x1 -> x0, blocking collectives: 41 us -> none  [body(): all_terms = lax.all_gather(own_terms.reshape(-1), SP)]
    dot_general x3 -> x0, matrix products: 20.2 us -> none  [the longest x1 7.75 us: body(): lax.dot_general(arrived_tokens, d_up, DOWNWARD, preferred_element_type=jn...]
    all_to_all x1 -> x0, waiting for transfers between devices: 18.3 us -> none  [body(): lax.all_to_all(both, 'ep', split_axis=0, concat_axis=0, tiled=True)]
    all_to_all x1 -> x0, starting transfers between devices: 12 us -> none  [body(): lax.all_to_all(both, 'ep', split_axis=0, concat_axis=0, tiled=True)]
    ppermute x2 -> x0, waiting for transfers between devices: 8.78 us -> none  [the longest x1 7.36 us: body(): pair_part = lax.ppermute(passed_on, 'pair', [(0, 1), (1, 0)])]
    all_to_all x1, starting transfers between devices: 3.75 us -> 9.96 us  [body(): lax.all_to_all(grad_mid, SP, split_axis=1, concat_axis=0, tiled=True)]
    unnamed x53 -> x51, local copies, waits for them, and re-layouts: 6.29 us -> 12.2 us
  transfers between devices with their start and end apart: 5 -> 2, of which waited for: 3 -> 0; matrix products, arithmetic and copies ran while one was open for 24% -> 17% of each run, Pallas kernels for 6% -> 12%
where the time goes in v2:
time: 243 us; the launch traced here: 242 us
  Pallas kernels  122 us (50%)
  matrix products  48.2 us (20%)
  local copies, waits for them, and re-layouts  34.4 us (14%)
  between operations  14.5 us (6%)
  starting transfers between devices  10 us (4%)
  other arithmetic  9.75 us (4%)
    pallas_call x1, Pallas kernels, dispatch_rows(): pl.pallas_call(functools.partial(dispatch_kernel, experts, width), out_sh...  53.1 us
    pallas_call x1, Pallas kernels, return_rows(): pl.pallas_call(functools.partial(return_kernel, experts, width, min(8, ex...  39.8 us
    pallas_call x1, Pallas kernels, suffix_states(): pl.pallas_call(functools.partial(suffix_kernel, count, rows), out_shape=(...  29.4 us
    unnamed x51, local copies, waits for them, and re-layouts  12.2 us
    all_to_all x1, starting transfers between devices, body(): lax.all_to_all(grad_mid, SP, split_axis=1, concat_axis=0, tiled=True)  9.96 us
    dot_general x1, matrix products, body(): jnp.dot(arrived_tokens, gate_mat, preferred_element_type=jnp.float32)  6.53 us
    dot_general x1, matrix products, body(): up_pre = jnp.dot(arrived_tokens, up_mat, preferred_element_type=jnp.float32)  5.31 us
    dot_general x1, matrix products, body(): lax.dot_general(d_up, up_mat, ACROSS, preferred_element_type=jnp.float32)  5.01 us
  transfers between devices with their start and end apart: 2, of which 0 were waited for; matrix products, arithmetic and copies ran while one was open for 17% of the time, Pallas kernels for 12%

profile of v2, /device:TPU:0, one launch (start us, length us, event | category | flops | bytes accessed | tf_op | source)
XLA Modules:
  0.0 242.2 jit_solution(13476946105849944110)
XLA Ops:
  11.3 1.3 mul.208
  12.7 1.9 mul.209
  14.9 2.2 convolution_convert_fusion.1
  17.1 1.3 convolution_convert_fusion
  18.4 53.1 %dispatch_rows.1 = (bf16[2,8,48,2048]{3,2,1,0:T(8,128)(2,1)}, bf16[2,8,48,2048]{3,2,1,0:T(8,128)(2,1)}) custom-call(bf16[8,48,1024]{2,1,0:T(8,128)(2,1)} %bitcast.227, bf16[8,48,1024]{2,1,0:T(8,128)(2,1)} %bitcast.228), custom_call_target="tpu_custom_call" | custom-call | tf_op jit(solution)/shard_map/dispatch_rows/pallas_call | solution.py:131
  71.6 6.5 %fusion.30 = f32[768,896]{1,0:T(8,128)S(1)} fusion(bf16[768,2048]{1,0:T(8,128)(2,1)} %bitcast.229, bf16[1,2048,896]{2,1,0:T(8,128)(2,1)} %param.20), kind=kOutput, calls=%fused_computation.57 | convolution fusion | flops 2818572288 | bytes 9568256 | tf_op jit(solution)/shard_map/dot_general | solution.py:516
  78.2 3.5 %fusion.36 = f32[768,896]{1,0:T(8,128)S(1)} fusion(bf16[768,2048]{1,0:T(8,128)(2,1)S(1)} %bitcast.233, bf16[1,896,2048]{2,1,0:T(8,128)(2,1)S(1)} %copy-done.19), kind=kOutput, calls=%fused_computation.63 | convolution fusion | flops 2818572288 | bytes 9568256 | tf_op jit(solution)/shard_map/dot_general | solution.py:520
  81.8 5.3 %multiply_convert_fusion = (bf16[768,896]{1,0:T(8,128)(2,1)}, bf16[768,896]{1,0:T(8,128)(2,1)S(1)}, bf16[768,896]{1,0:T(8,128)(2,1)S(1)}) fusion(f32[768,896]{1,0:T(8,128)S(1)} %fusion.30, f32[768,896]{1,0:T(8,128)S(1)} %fusion.36, bf16[768,2048]{1,0:T(8,128)(2,1)S(1)} %bitcast.231, bf16[1,2048,896]{2,1,0:T(8,128)(2,1)S(1)} %copy-done.21), kind=kOutput, calls=%fused_computation.65 | convolution fusion | flops 2829582336 | bytes 16449536 | tf_op jit(solution)/shard_map/dot_general | solution.py:517
  87.1 3.4 %fusion.28 = f32[768,2048]{1,0:T(8,128)S(1)} fusion(bf16[768,896]{1,0:T(8,128)(2,1)S(1)} %get-tuple-element.420.d_gate, bf16[1,2048,896]{2,1,0:T(8,128)(2,1)S(1)} %copy-done.20), kind=kOutput, calls=%fused_computation.55 | convolution fusion | flops 2818572288 | bytes 11337728 | tf_op jit(solution)/shard_map/dot_general | solution.py:525
  90.5 5.0 %add_convert_fusion = bf16[768,2048]{1,0:T(8,128)(2,1)} fusion(f32[768,2048]{1,0:T(8,128)S(1)} %fusion.28, bf16[768,896]{1,0:T(8,128)(2,1)S(1)} %get-tuple-element.421.d_up, bf16[1,2048,896]{2,1,0:T(8,128)(2,1)S(1)} %copy-done.21), kind=kOutput, calls=%fused_computation.54 | convolution fusion | flops 2821718016 | bytes 14483456 | tf_op jit(solution)/shard_map/dot_general | solution.py:527
  95.6 39.8 %return_rows.1 = (bf16[8,48,1024]{2,1,0:T(8,128)(2,1)}, bf16[2048,896]{1,0:T(8,128)(2,1)}, bf16[2048,896]{1,0:T(8,128)(2,1)}, bf16[896,2048]{1,0:T(8,128)(2,1)}) custom-call(bf16[2,8,48,2048]{3,2,1,0:T(8,128)(2,1)} %bitcast.234, bf16[768,2048]{1,0:T(8,128)(2,1)} %bitcast.230, bf16[768,2048]{1,0:T(8,128)(2,1)} %bitcast.232, ...), custom_call_target="tpu_custom_call" | custom-call | tf_op jit(solution)/shard_map/return_rows/pallas_call | solution.py:405
  135.4 1.5 fusion.40
  136.9 2.2 all_gather.6
  140.0 10.0 %all-to-all-start = ((bf16[128,16,128]{2,0,1:T(8,128)(2,1)}), bf16[128,16,128]{2,0,1:T(8,128)(2,1)}, u32[]{:S(2)}, u32[]{:S(2)}) async-start(bf16[128,16,128]{2,0,1:T(8,128)(2,1)} %copy_bitcast_fusion.8), calls=%async_computation | async-start | bytes 1048576 | tf_op jit(solution)/shard_map/all_to_all | solution.py:542
  158.6 18.9 %while.23 = (s32[]{:T(128)}, f32[4,64,128]{2,1,0:T(8,128)S(1)}, bf16[2,64,4,64]{1,3,2,0:T(8,128)(2,1)}, f32[2,64,4,64]{1,3,0,2:T(8,128)}, f32[2,64,4,128]{3,1,0,...) while((s32[]{:T(128)}, f32[4,64,128]{2,1,0:T(8,128)S(1)}, ...), condition=%wide.region_6.7_spmd.clone, body=%wide.region_4.6_spmd.clone.sunk | while | flops 190324736 | bytes 5430457 | solution.py:561
  180.2 1.8 fusion.50
  183.8 29.4 %suffix_states.1 = (f32[16,16,128]{2,1,0:T(8,128)}, f32[2,128]{1,0:T(2,128)}) custom-call(f32[16,2,16,128]{3,2,1,0:T(8,128)} %pad_maximum_fusion.state, f32[16,16,128]{2,1,0:T(8,128)} %bitcast.238, f32[2,128]{1,0:T(2,128)} %reshape.184.terms), custom_call_target="tpu_custom_call" | custom-call | tf_op jit(solution)/shard_map/suffix_states/pallas_call | solution.py:250
  213.2 2.3 copy_subtract_fusion
  217.2 1.3 fusion.57
  222.8 2.2 convolution_bitcast_fusion.4
  225.9 4.3 %copy.220 = bf16[1,2048,896]{2,1,0:T(8,128)(2,1)} copy(bf16[1,2048,896]{2,1,0:T(8,128)(2,1)} %bitcast.226) | data formatting | bytes 7340032
  230.2 1.9 copy.221
  232.0 1.5 copy-done.1
  233.5 1.8 copy.222
  (143 shorter events, 43.7 us)
Async XLA Ops:
  7.2 144.2 %copy-start = (bf16[512,2048]{1,0:T(8,128)(2,1)S(1)}, bf16[512,2048]{1,0:T(8,128)(2,1)}, u32[]{:S(2)}) copy-start(bf16[512,2048]{1,0:T(8,128)(2,1)} %param.24) | copy-start | bytes 6291460
  7.2 7.4 %copy-start.17 = (f32[128,2]{0,1:T(2,128)S(1)}, f32[128,2]{0,1:T(2,128)}, u32[]{:S(2)}) copy-start(f32[128,2]{0,1:T(2,128)} %param.19) | copy-start | bytes 3076
  71.6 6.6 %copy-start.4 = (bf16[2,8,48,2048]{3,2,1,0:T(8,128)(2,1)S(1)}, bf16[2,8,48,2048]{3,2,1,0:T(8,128)(2,1)}, u32[]{:S(2)}) copy-start(bf16[2,8,48,2048]{3,2,1,0:T(8,128)(2,1)} %get-tuple-element.256) | copy-start | bytes 9437188
  71.6 6.6 %copy-start.19 = (bf16[1,896,2048]{2,1,0:T(8,128)(2,1)S(1)}, bf16[1,896,2048]{2,1,0:T(8,128)(2,1)}, u32[]{:S(2)}) copy-start(bf16[1,896,2048]{2,1,0:T(8,128)(2,1)} %param.22) | copy-start | bytes 11010052
  78.1 3.6 %copy-start.3 = (bf16[2,8,48,2048]{3,2,1,0:T(8,128)(2,1)S(1)}, bf16[2,8,48,2048]{3,2,1,0:T(8,128)(2,1)}, u32[]{:S(2)}) copy-start(bf16[2,8,48,2048]{3,2,1,0:T(8,128)(2,1)} %get-tuple-element.257) | copy-start | bytes 9437188
  78.2 3.6 %copy-start.21 = (bf16[1,2048,896]{2,1,0:T(8,128)(2,1)S(1)}, bf16[1,2048,896]{2,1,0:T(8,128)(2,1)}, u32[]{:S(2)}) copy-start(bf16[1,2048,896]{2,1,0:T(8,128)(2,1)} %param.21) | copy-start | bytes 11010052
  81.7 5.3 %copy-start.20 = (bf16[1,2048,896]{2,1,0:T(8,128)(2,1)S(1)}, bf16[1,2048,896]{2,1,0:T(8,128)(2,1)}, u32[]{:S(2)}) copy-start(bf16[1,2048,896]{2,1,0:T(8,128)(2,1)} %param.20) | copy-start | bytes 11010052
  87.1 3.5 %copy-start.8 = (bf16[768,896]{1,0:T(8,128)(2,1)}, bf16[768,896]{1,0:T(8,128)(2,1)S(1)}, u32[]{:S(2)}) copy-start(bf16[768,896]{1,0:T(8,128)(2,1)S(1)} %get-tuple-element.420.d_gate) | copy-start | bytes 4128772
  87.1 3.5 %copy-start.9 = (bf16[768,896]{1,0:T(8,128)(2,1)}, bf16[768,896]{1,0:T(8,128)(2,1)S(1)}, u32[]{:S(2)}) copy-start(bf16[768,896]{1,0:T(8,128)(2,1)S(1)} %get-tuple-element.421.d_up) | copy-start | bytes 4128772
  95.5 39.8 %copy-start.10 = (bf16[128,2048]{1,0:T(8,128)(2,1)S(1)}, bf16[128,2048]{1,0:T(8,128)(2,1)}, u32[]{:S(2)}) copy-start(bf16[128,2048]{1,0:T(8,128)(2,1)} %param.17) | copy-start | bytes 1572868
  139.0 14.0 %copy-start.14 = (bf16[128,512]{1,0:T(8,128)(2,1)S(1)}, bf16[128,512]{1,0:T(8,128)(2,1)}, u32[]{:S(2)}) copy-start(bf16[128,512]{1,0:T(8,128)(2,1)} %param.27) | copy-start | bytes 393220
  140.0 13.8 %copy-start.13 = (f32[128,256]{1,0:T(8,128)S(1)}, f32[128,256]{1,0:T(8,128)}, u32[]{:S(2)}) copy-start(f32[128,256]{1,0:T(8,128)} %param.28) | copy-start | bytes 393220
  140.0 14.7 %copy-start.15 = (bf16[128,256]{1,0:T(8,128)(2,1)S(1)}, bf16[128,256]{1,0:T(8,128)(2,1)}, u32[]{:S(2)}) copy-start(bf16[128,256]{1,0:T(8,128)(2,1)} %param.26) | copy-start | bytes 196612
  140.0 82.8 %all-to-all-start = ((bf16[128,16,128]{2,0,1:T(8,128)(2,1)}), bf16[128,16,128]{2,0,1:T(8,128)(2,1)}, u32[]{:S(2)}, u32[]{:S(2)}) async-start(bf16[128,16,128]{2,0,1:T(8,128)(2,1)} %copy_bitcast_fusion.8), calls=%async_computation | async-start | bytes 1048576 | tf_op jit(solution)/shard_map/all_to_all | solution.py:542
  149.9 5.6 %copy-start.16 = (bf16[128,256]{1,0:T(8,128)(2,1)S(1)}, bf16[128,256]{1,0:T(8,128)(2,1)}, u32[]{:S(2)}) copy-start(bf16[128,256]{1,0:T(8,128)(2,1)} %param.25) | copy-start | bytes 196612
  150.0 72.8 %all-gather.2.cloned.1.call-start = ((), (), s32[]{:S(2)}) async-start(), calls=%async_computation.1 | async-start | bytes 2228224 | tf_op jit(solution)/shard_map/all_gather | solution.py:541
  153.0 5.6 %copy-start.6 = (bf16[2,64,4,128]{3,2,1,0:T(4,128)(2,1)}, bf16[2,64,4,128]{3,2,1,0:T(4,128)(2,1)S(1)}, u32[]{:S(2)}) copy-start(bf16[2,64,4,128]{3,2,1,0:T(4,128)(2,1)S(1)} %reshape.181) | copy-start | bytes 393220
  177.5 5.4 %copy-start.5 = (f32[2,64,4,64]{1,3,2,0:T(8,128)S(1)}, f32[2,64,4,64]{1,3,2,0:T(8,128)}, u32[]{:S(2)}) copy-start(f32[2,64,4,64]{1,3,2,0:T(8,128)} %get-tuple-element.262) | copy-start | bytes 393220
  177.6 35.6 %copy-start.7 = (bf16[2,64,4,128]{3,2,1,0:T(4,128)(2,1)S(1)}, bf16[2,64,4,128]{3,2,1,0:T(4,128)(2,1)}, u32[]{:S(2)}) copy-start(bf16[2,64,4,128]{3,2,1,0:T(4,128)(2,1)} %copy-done.6) | copy-start | bytes 393220
  213.2 8.0 %copy-start.11 = (bf16[2,64,4,64]{1,3,2,0:T(8,128)(2,1)S(1)}, bf16[2,64,4,64]{1,3,2,0:T(8,128)(2,1)}, u32[]{:S(2)}) copy-start(bf16[2,64,4,64]{1,3,2,0:T(8,128)(2,1)} %get-tuple-element.259) | copy-start | bytes 196612
  213.2 8.9 %copy-start.18 = (f32[2,128]{1,0:T(2,128)S(1)}, f32[2,128]{1,0:T(2,128)}, u32[]{:S(2)}) copy-start(f32[2,128]{1,0:T(2,128)} %get-tuple-element.265) | copy-start | bytes 3076
  215.5 4.7 %copy-start.12 = (bf16[2,64,4,64]{1,3,0,2:T(8,128)(2,1)S(1)}, bf16[2,64,4,64]{1,3,0,2:T(8,128)(2,1)}, u32[]{:S(2)}) copy-start(bf16[2,64,4,64]{1,3,0,2:T(8,128)(2,1)} %get-tuple-element.423) | copy-start | bytes 196612
  225.9 4.3 %copy-start.2 = (bf16[2048,896]{1,0:T(8,128)(2,1)S(1)}, bf16[2048,896]{1,0:T(8,128)(2,1)}, u32[]{:S(2)}) copy-start(bf16[2048,896]{1,0:T(8,128)(2,1)} %get-tuple-element.267) | copy-start | bytes 11010052
  230.2 3.4 %copy-start.1 = (bf16[896,2048]{1,0:T(8,128)(2,1)S(1)}, bf16[896,2048]{1,0:T(8,128)(2,1)}, u32[]{:S(2)}) copy-start(bf16[896,2048]{1,0:T(8,128)(2,1)} %get-tuple-element.268) | copy-start | bytes 11010052
Sparse Core Ops, SparseCore 0:
  153.5 62.7 all-gather.1

commit v3 on v2

--- a/solution.py
+++ b/solution.py
@@ -274,10 +274,11 @@
 
 
 def return_kernel(
-    experts, width, steps, parts, tokens, grads, hidden, d_gate, d_up,
-    returned, gate_out, up_out, down_out,
+    experts, width, steps, parts, tokens, grads, hidden, d_gate, d_up, mixer,
+    returned, mixer_all, gate_out, up_out, down_out,
     core_held, pair_stage, pair_held, send_stage, gate_stage, up_stage, down_stage,
     out_sem, local_sem, core_send, core_recv, pair_send, pair_recv, back_send, back_recv,
+    mix_send, mix_recv, over_send, over_recv,
 ):
     e, p, t = lax.axis_index("ep"), lax.axis_index("pair"), lax.axis_index("tp")
     barrier = pltpu.get_barrier_semaphore()
@@ -316,6 +317,32 @@
             src_ref=send_stage.at[k], dst_ref=returned.at[e], send_sem=back_send.at[k],
             recv_sem=back_recv.at[k], device_id=(owner(k), p, t), device_id_type=MESH,
         )
+
+    def mix_copy(k):
+        return pltpu.make_async_remote_copy(
+            src_ref=mixer, dst_ref=mixer_all.at[e, p], send_sem=mix_send.at[k],
+            recv_sem=mix_recv.at[k], device_id=(owner(k), p, t), device_id_type=MESH,
+        )
+
+    def from_owner(k):
+        return lax.rem(e - 1 - k + 2 * experts, experts)
+
+    def mix_landed(k):
+        place = mixer_all.at[from_owner(k), p]
+        return pltpu.make_async_remote_copy(
+            src_ref=place, dst_ref=place, send_sem=mix_send.at[k], recv_sem=mix_recv.at[k],
+            device_id=(from_owner(k), p, t), device_id_type=MESH,
+        )
+
+    def over_copy(k, side):
+        place = mixer_all.at[from_owner(k), side]
+        return pltpu.make_async_remote_copy(
+            src_ref=place, dst_ref=place, send_sem=over_send.at[k], recv_sem=over_recv.at[k],
+            device_id=(e, 1 - p, t), device_id_type=MESH,
+        )
+
+    mix_own = pltpu.make_async_copy(mixer, mixer_all.at[e, p], mix_recv.at[experts - 1])
+    mix_own.start()
 
     def half_of(which, k):
         side = 1 - p if which == 0 else p
@@ -331,6 +358,8 @@
         if k:
             pair_copy(k - 1).start()
     pair_copy(experts - 1).start()
+    for k in range(experts - 1):
+        mix_copy(k).start()
     for k in range(experts):
         core_copy(1, k).wait_recv()
 
@@ -366,6 +395,14 @@
             def _():
                 back_copy(k).start()
 
+        for j in range(each):
+            k = i * each + j
+
+            @pl.when(k < experts - 1)
+            def _():
+                mix_landed(k).wait_recv()
+                over_copy(k, p).start()
+
         pltpu.make_async_copy(gate_stage.at[cut], gate_out.at[cut], out_sem.at[1]).start()
         pltpu.make_async_copy(up_stage.at[cut], up_out.at[cut], out_sem.at[2]).start()
         return carry
@@ -374,6 +411,8 @@
     own = pltpu.make_async_copy(send_stage.at[experts - 1], returned.at[e], local_sem)
     own.start()
     own.wait()
+    mix_own.wait()
+    over_copy(experts - 1, p).start()
     for k in range(experts - 1):
         source = lax.rem(e - 1 - k + experts, experts)
         pltpu.make_async_remote_copy(
@@ -384,14 +423,17 @@
         core_copy(0, k).wait_send()
         core_copy(1, k).wait_send()
         pair_copy(k).wait_send()
+        over_copy(k, 1 - p).wait_recv()
+        over_copy(k, p).wait_send()
         if k < experts - 1:
             back_copy(k).wait_send()
+            mix_copy(k).wait_send()
     pltpu.make_async_copy(down_stage, down_out, out_sem.at[0]).wait()
     pltpu.make_async_copy(gate_stage, gate_out, out_sem.at[1]).wait()
     pltpu.make_async_copy(up_stage, up_out, out_sem.at[2]).wait()
 
 
-def return_rows(parts, tokens, grads, hidden, d_gate, d_up):
+def return_rows(parts, tokens, grads, hidden, d_gate, d_up, mixer):
     _, experts, capacity, model_width = parts.shape
     width = model_width // 2
     units = hidden.shape[1]
@@ -404,9 +446,9 @@
     shape = jax.ShapeDtypeStruct
     return pl.pallas_call(
         functools.partial(return_kernel, experts, width, min(8, experts)),
-        out_shape=(shape(half, kind), shape(wide, kind), shape(wide, kind), shape(tall, kind)),
-        in_specs=[vmem] * 6,
-        out_specs=(vmem, hbm, hbm, hbm),
+        out_shape=(shape(half, kind), shape((experts, 2) + mixer.shape, kind), shape(wide, kind), shape(wide, kind), shape(tall, kind)),
+        in_specs=[vmem] * 7,
+        out_specs=(vmem, vmem, hbm, hbm, hbm),
         scratch_shapes=[
             pltpu.VMEM((2,) + half, kind),
             pltpu.VMEM(half, kind),
@@ -423,12 +465,16 @@
             dma((experts,)),
             dma((experts,)),
             dma((experts,)),
+            dma((experts,)),
+            dma((experts,)),
+            dma((experts,)),
+            dma((experts,)),
         ],
         compiler_params=pltpu.CompilerParams(
             collective_id=2, has_side_effects=True, vmem_limit_bytes=60 * 1024 * 1024
         ),
         name="return_rows",
-    )(parts, tokens, grads, hidden, d_gate, d_up)
+    )(parts, tokens, grads, hidden, d_gate, d_up, mixer)
 
 
 def block_back(carried, inputs):
@@ -526,19 +572,20 @@
         d_gate, gate_mat, ACROSS, preferred_element_type=jnp.float32
     ) + lax.dot_general(d_up, up_mat, ACROSS, preferred_element_type=jnp.float32)
     parts = partial_value.astype(jnp.bfloat16)
-    returned, grad_gate, grad_up, grad_down = return_rows(
+    returned, mixer_all, grad_gate, grad_up, grad_down = return_rows(
         parts.reshape(2, experts, capacity, model_width),
         arrived_tokens,
         arrived_grads,
         hidden,
         d_gate,
         d_up,
+        mixer_out,
     )
     returned = returned.reshape(experts * capacity, col_count)
     moe_grad = lax.dot_general(token_pick, returned, DOWNWARD, preferred_element_type=jnp.float32)
     grad_mid = (source_grads.astype(jnp.float32) + moe_grad).astype(jnp.bfloat16)
     grad_mid = lax.all_gather(grad_mid, "tp", axis=1, tiled=True)
-    mixer_all = lax.all_gather(mixer_out, SP, axis=0, tiled=True)
+    mixer_all = mixer_all.reshape(sp_count * tok_rows, -1)
     mid_columns = lax.all_to_all(grad_mid, SP, split_axis=1, concat_axis=0, tiled=True)
     grad_out_weight = lax.dot_general(
         mixer_all, mid_columns, DOWNWARD, preferred_element_type=jnp.float32
@@ -559,7 +606,7 @@
     inputs = (q_blocks, k_blocks, v_blocks, shaped(grad_mixed, DV), decay_blocks, block_states)
     zero_state = jnp.zeros((heads_local, DK, DV), jnp.float32)
     local_sum, (grad_q, grad_k, grad_v, contrib) = lax.scan(
-        block_back, zero_state, inputs, reverse=True
+        block_back, zero_state, inputs, reverse=True, unroll=True
     )
     cumul = jnp.cumsum(decay_blocks, axis=1)
     totals = cumul[:, -1]

time: 243 us -> 244 us (level)
  Pallas kernels: 122 us -> 137 us
  between operations: 14.5 us -> 1.17 us
  matrix products: 48.2 us -> 54.9 us
  local copies, waits for them, and re-layouts: 34.4 us -> 28 us
    pallas_call x1, Pallas kernels: 39.8 us -> 59.3 us  [return_rows(): pl.pallas_call(functools.partial(return_kernel, experts, width, min(8, ex...]
    pallas_call x1, Pallas kernels: 29.4 us -> 24.5 us  [suffix_states(): pl.pallas_call(functools.partial(suffix_kernel, count, rows), out_shape=(...]
    dynamic_slice x8 -> x0, local copies, waits for them, and re-layouts: 4.36 us -> none  [body(): lax.scan(block_back, zero_state, inputs, reverse=True)]
    unnamed x51 -> x52, local copies, waits for them, and re-layouts: 12.2 us -> 12 us
  transfers between devices with their start and end apart: 2 -> 1, of which waited for: 0 -> 0; matrix products, arithmetic and copies ran while one was open for 17% -> 17% of each run, Pallas kernels for 12% -> 10%
where the time goes in v3:
time: 244 us; the launch traced here: 243 us
  Pallas kernels  137 us (56%)
  matrix products  54.9 us (22%)
  local copies, waits for them, and re-layouts  28 us (11%)
  starting transfers between devices  12 us (5%)
  other arithmetic  7.71 us (3%)
    pallas_call x1, Pallas kernels, return_rows(): pl.pallas_call(functools.partial(return_kernel, experts, width, min(8, ex...  59.3 us
    pallas_call x1, Pallas kernels, dispatch_rows(): pl.pallas_call(functools.partial(dispatch_kernel, experts, width), out_sh...  53.1 us
    pallas_call x1, Pallas kernels, suffix_states(): pl.pallas_call(functools.partial(suffix_kernel, count, rows), out_shape=(...  24.5 us
    all_to_all x1, starting transfers between devices, body(): lax.all_to_all(grad_mid, SP, split_axis=1, concat_axis=0, tiled=True)  12 us
    unnamed x52, local copies, waits for them, and re-layouts  12 us
    dot_general x1, matrix products, body(): jnp.dot(arrived_tokens, gate_mat, preferred_element_type=jnp.float32)  6.53 us
    dot_general x1, matrix products, body(): up_pre = jnp.dot(arrived_tokens, up_mat, preferred_element_type=jnp.float32)  5.3 us
    dot_general x1, matrix products, body(): lax.dot_general(d_up, up_mat, ACROSS, preferred_element_type=jnp.float32)  5.01 us
  transfers between devices with their start and end apart: 1, of which 0 were waited for; matrix products, arithmetic and copies ran while one was open for 17% of the time, Pallas kernels for 10%

profile of v3, /device:TPU:0, one launch (start us, length us, event | category | flops | bytes accessed | tf_op | source)
XLA Modules:
  0.0 242.9 jit_solution(17266949840434952554)
XLA Ops:
  4.8 1.3 mul.177
  6.1 1.9 mul.178
  8.4 2.2 convolution_convert_fusion.1
  10.5 1.3 convolution_convert_fusion
  11.9 53.1 %dispatch_rows.1 = (bf16[2,8,48,2048]{3,2,1,0:T(8,128)(2,1)}, bf16[2,8,48,2048]{3,2,1,0:T(8,128)(2,1)}) custom-call(bf16[8,48,1024]{2,1,0:T(8,128)(2,1)} %bitcast.202, bf16[8,48,1024]{2,1,0:T(8,128)(2,1)} %bitcast.203), custom_call_target="tpu_custom_call" | custom-call | tf_op jit(solution)/shard_map/dispatch_rows/pallas_call | solution.py:131
  65.0 6.5 %fusion.2 = f32[768,896]{1,0:T(8,128)S(1)} fusion(bf16[768,2048]{1,0:T(8,128)(2,1)} %bitcast.204, bf16[1,2048,896]{2,1,0:T(8,128)(2,1)} %param.18), kind=kOutput, calls=%fused_computation.3 | convolution fusion | flops 2818572288 | bytes 9568256 | tf_op jit(solution)/shard_map/dot_general | solution.py:562
  71.6 3.5 %fusion.8 = f32[768,896]{1,0:T(8,128)S(1)} fusion(bf16[768,2048]{1,0:T(8,128)(2,1)S(1)} %bitcast.208, bf16[1,896,2048]{2,1,0:T(8,128)(2,1)S(1)} %copy-done.19), kind=kOutput, calls=%fused_computation.9 | convolution fusion | flops 2818572288 | bytes 9568256 | tf_op jit(solution)/shard_map/dot_general | solution.py:566
  75.2 5.3 %multiply_convert_fusion = (bf16[768,896]{1,0:T(8,128)(2,1)}, bf16[768,896]{1,0:T(8,128)(2,1)S(1)}, bf16[768,896]{1,0:T(8,128)(2,1)S(1)}) fusion(f32[768,896]{1,0:T(8,128)S(1)} %fusion.2, f32[768,896]{1,0:T(8,128)S(1)} %fusion.8, bf16[768,2048]{1,0:T(8,128)(2,1)S(1)} %bitcast.206, bf16[1,2048,896]{2,1,0:T(8,128)(2,1)S(1)} %copy-done.21), kind=kOutput, calls=%fused_computation.11 | convolution fusion | flops 2829582336 | bytes 16449536 | tf_op jit(solution)/shard_map/dot_general | solution.py:563
  80.5 3.5 %fusion = f32[768,2048]{1,0:T(8,128)S(1)} fusion(bf16[768,896]{1,0:T(8,128)(2,1)S(1)} %get-tuple-element.31.d_gate, bf16[1,2048,896]{2,1,0:T(8,128)(2,1)S(1)} %copy-done.20), kind=kOutput, calls=%fused_computation.1 | convolution fusion | flops 2818572288 | bytes 11337728 | tf_op jit(solution)/shard_map/dot_general | solution.py:571
  84.0 5.0 %add_convert_fusion = bf16[768,2048]{1,0:T(8,128)(2,1)} fusion(f32[768,2048]{1,0:T(8,128)S(1)} %fusion, bf16[768,896]{1,0:T(8,128)(2,1)S(1)} %get-tuple-element.32.d_up, bf16[1,2048,896]{2,1,0:T(8,128)(2,1)S(1)} %copy-done.21), kind=kOutput, calls=%fused_computation | convolution fusion | flops 2821718016 | bytes 14483456 | tf_op jit(solution)/shard_map/dot_general | solution.py:573
  89.0 59.3 %return_rows.1 = (bf16[8,48,1024]{2,1,0:T(8,128)(2,1)}, bf16[8,2,128,512]{3,2,1,0:T(8,128)(2,1)}, bf16[2048,896]{1,0:T(8,128)(2,1)}, bf16[2048,896]{1,0:T(8,128)(2,1)}, bf16[896,2048]{1,0:T(8,128)(2,1)}) custom-call(bf16[2,8,48,2048]{3,2,1,0:T(8,128)(2,1)} %bitcast.209, bf16[768,2048]{1,0:T(8,128)(2,1)} %bitcast.205, bf16[768,2048]{1,0:T(8,128)(2,1)} %bitcast.207, ...), custom_call_target="tpu_custom_call" | custom-call | tf_op jit(solution)/shard_map/return_rows/pallas_call | solution.py:447
  148.3 1.5 fusion.12
  149.8 2.3 all_gather.3
  153.1 12.0 %all-to-all-start = ((bf16[128,16,128]{2,0,1:T(8,128)(2,1)}), bf16[128,16,128]{2,0,1:T(8,128)(2,1)}, u32[]{:S(2)}, u32[]{:S(2)}) async-start(bf16[128,16,128]{2,0,1:T(8,128)(2,1)} %copy_bitcast_fusion), calls=%async_computation | async-start | bytes 1048576 | tf_op jit(solution)/shard_map/all_to_all | solution.py:589
  178.8 1.7 fusion.23
  187.0 2.0 fusion.93
  191.9 1.9 fusion.47
  193.8 24.5 %suffix_states.1 = (f32[16,16,128]{2,1,0:T(8,128)}, f32[2,128]{1,0:T(2,128)}) custom-call(f32[16,2,16,128]{3,2,1,0:T(8,128)} %pad_maximum_fusion.state, f32[16,16,128]{2,1,0:T(8,128)} %bitcast.214, f32[2,128]{1,0:T(2,128)} %reduce_sum.56.terms), custom_call_target="tpu_custom_call" | custom-call | tf_op jit(solution)/shard_map/suffix_states/pallas_call | solution.py:250
  218.3 2.1 maximum_subtract_fusion
  230.3 3.1 %fusion.105 = f32[512,128]{1,0:T(8,128)} fusion(bf16[2048,512]{1,0:T(8,128)(2,1)} %bitcast.210, bf16[2048,128]{1,0:T(8,128)(2,1)} %bitcast.45), kind=kOutput, calls=%fused_computation.162 | convolution fusion | flops 268435456 | bytes 2883584 | tf_op jit(solution)/shard_map/dot_general | solution.py:590
  233.4 4.3 %copy.350 = bf16[1,2048,896]{2,1,0:T(8,128)(2,1)} copy(bf16[1,2048,896]{2,1,0:T(8,128)(2,1)} %bitcast.201) | data formatting | bytes 7340032
  237.7 1.9 copy.351
  239.6 1.5 copy-done.1
  241.1 1.8 copy.352
  (124 shorter events, 38.0 us)
Async XLA Ops:
  0.6 170.9 %copy-start = (bf16[512,2048]{1,0:T(8,128)(2,1)S(1)}, bf16[512,2048]{1,0:T(8,128)(2,1)}, u32[]{:S(2)}) copy-start(bf16[512,2048]{1,0:T(8,128)(2,1)} %param.22) | copy-start | bytes 6291460
  0.6 7.4 %copy-start.17 = (f32[128,2]{0,1:T(2,128)S(1)}, f32[128,2]{0,1:T(2,128)}, u32[]{:S(2)}) copy-start(f32[128,2]{0,1:T(2,128)} %param.17) | copy-start | bytes 3076
  65.0 6.6 %copy-start.4 = (bf16[2,8,48,2048]{3,2,1,0:T(8,128)(2,1)S(1)}, bf16[2,8,48,2048]{3,2,1,0:T(8,128)(2,1)}, u32[]{:S(2)}) copy-start(bf16[2,8,48,2048]{3,2,1,0:T(8,128)(2,1)} %get-tuple-element.17) | copy-start | bytes 9437188
  65.0 6.6 %copy-start.19 = (bf16[1,896,2048]{2,1,0:T(8,128)(2,1)S(1)}, bf16[1,896,2048]{2,1,0:T(8,128)(2,1)}, u32[]{:S(2)}) copy-start(bf16[1,896,2048]{2,1,0:T(8,128)(2,1)} %param.20) | copy-start | bytes 11010052
  71.6 3.6 %copy-start.3 = (bf16[2,8,48,2048]{3,2,1,0:T(8,128)(2,1)S(1)}, bf16[2,8,48,2048]{3,2,1,0:T(8,128)(2,1)}, u32[]{:S(2)}) copy-start(bf16[2,8,48,2048]{3,2,1,0:T(8,128)(2,1)} %get-tuple-element.18) | copy-start | bytes 9437188
  71.6 3.6 %copy-start.21 = (bf16[1,2048,896]{2,1,0:T(8,128)(2,1)S(1)}, bf16[1,2048,896]{2,1,0:T(8,128)(2,1)}, u32[]{:S(2)}) copy-start(bf16[1,2048,896]{2,1,0:T(8,128)(2,1)} %param.19) | copy-start | bytes 11010052
  75.2 5.3 %copy-start.20 = (bf16[1,2048,896]{2,1,0:T(8,128)(2,1)S(1)}, bf16[1,2048,896]{2,1,0:T(8,128)(2,1)}, u32[]{:S(2)}) copy-start(bf16[1,2048,896]{2,1,0:T(8,128)(2,1)} %param.18) | copy-start | bytes 11010052
  80.5 3.5 %copy-start.5 = (bf16[768,896]{1,0:T(8,128)(2,1)}, bf16[768,896]{1,0:T(8,128)(2,1)S(1)}, u32[]{:S(2)}) copy-start(bf16[768,896]{1,0:T(8,128)(2,1)S(1)} %get-tuple-element.31.d_gate) | copy-start | bytes 4128772
  80.5 3.5 %copy-start.6 = (bf16[768,896]{1,0:T(8,128)(2,1)}, bf16[768,896]{1,0:T(8,128)(2,1)S(1)}, u32[]{:S(2)}) copy-start(bf16[768,896]{1,0:T(8,128)(2,1)S(1)} %get-tuple-element.32.d_up) | copy-start | bytes 4128772
  89.0 59.3 %copy-start.13 = (bf16[128,2048]{1,0:T(8,128)(2,1)S(1)}, bf16[128,2048]{1,0:T(8,128)(2,1)}, u32[]{:S(2)}) copy-start(bf16[128,2048]{1,0:T(8,128)(2,1)} %param.15) | copy-start | bytes 1572868
  148.3 16.9 %copy-start.12 = (f32[128,256]{1,0:T(8,128)S(1)}, f32[128,256]{1,0:T(8,128)}, u32[]{:S(2)}) copy-start(f32[128,256]{1,0:T(8,128)} %param.26) | copy-start | bytes 393220
  149.8 18.8 %copy-start.9 = (bf16[128,256]{1,0:T(8,128)(2,1)S(1)}, bf16[128,256]{1,0:T(8,128)(2,1)}, u32[]{:S(2)}) copy-start(bf16[128,256]{1,0:T(8,128)(2,1)} %param.24) | copy-start | bytes 196612
  149.8 20.4 %copy-start.14 = (bf16[128,512]{1,0:T(8,128)(2,1)S(1)}, bf16[128,512]{1,0:T(8,128)(2,1)}, u32[]{:S(2)}) copy-start(bf16[128,512]{1,0:T(8,128)(2,1)} %param.25) | copy-start | bytes 393220
  153.1 77.2 %all-to-all-start = ((bf16[128,16,128]{2,0,1:T(8,128)(2,1)}), bf16[128,16,128]{2,0,1:T(8,128)(2,1)}, u32[]{:S(2)}, u32[]{:S(2)}) async-start(bf16[128,16,128]{2,0,1:T(8,128)(2,1)} %copy_bitcast_fusion), calls=%async_computation | async-start | bytes 1048576 | tf_op jit(solution)/shard_map/all_to_all | solution.py:589
  165.1 10.6 %copy-start.7 = (f32[64,64]{1,0:T(8,128)}, f32[64,64]{1,0:T(8,128)S(1)}, u32[]{:S(2)}) copy-start(f32[64,64]{1,0:T(8,128)S(1)} %fusion.81) | copy-start | bytes 49156
  170.8 6.0 %copy-start.11 = (bf16[8,4,8,128]{3,2,1,0:T(8,128)(2,1)}, bf16[8,4,8,128]{3,2,1,0:T(8,128)(2,1)S(1)}, u32[]{:S(2)}) copy-start(bf16[8,4,8,128]{3,2,1,0:T(8,128)(2,1)S(1)} %get-tuple-element.41) | copy-start | bytes 196612
  172.4 8.2 %copy-start.10 = (bf16[8,4,8,128]{3,2,1,0:T(8,128)(2,1)S(1)}, bf16[8,4,8,128]{3,2,1,0:T(8,128)(2,1)}, u32[]{:S(2)}) copy-start(bf16[8,4,8,128]{3,2,1,0:T(8,128)(2,1)} %get-tuple-element.42) | copy-start | bytes 196612
  180.5 9.1 %copy-start.16 = (f32[4,64]{1,0:T(4,128)S(1)}, f32[4,64]{1,0:T(4,128)}, u32[]{:S(2)}) copy-start(f32[4,64]{1,0:T(4,128)} %fusion.92) | copy-start | bytes 3076
  190.9 31.6 %copy-start.8 = (f32[64,64]{1,0:T(8,128)S(1)}, f32[64,64]{1,0:T(8,128)}, u32[]{:S(2)}) copy-start(f32[64,64]{1,0:T(8,128)} %copy-done.7) | copy-start | bytes 49156
  220.4 7.5 %copy-start.15 = (bf16[1,64,4,64]{3,1,2,0:T(8,128)(2,1)S(1)}, bf16[1,64,4,64]{3,1,2,0:T(8,128)(2,1)}, u32[]{:S(2)}) copy-start(bf16[1,64,4,64]{3,1,2,0:T(8,128)(2,1)} %get-tuple-element.35) | copy-start | bytes 98308
  221.7 7.9 %copy-start.18 = (f32[2,128]{1,0:T(2,128)S(1)}, f32[2,128]{1,0:T(2,128)}, u32[]{:S(2)}) copy-start(f32[2,128]{1,0:T(2,128)} %get-tuple-element.21) | copy-start | bytes 3076
  233.4 4.3 %copy-start.2 = (bf16[2048,896]{1,0:T(8,128)(2,1)S(1)}, bf16[2048,896]{1,0:T(8,128)(2,1)}, u32[]{:S(2)}) copy-start(bf16[2048,896]{1,0:T(8,128)(2,1)} %get-tuple-element.24) | copy-start | bytes 11010052
  237.7 3.4 %copy-start.1 = (bf16[896,2048]{1,0:T(8,128)(2,1)S(1)}, bf16[896,2048]{1,0:T(8,128)(2,1)}, u32[]{:S(2)}) copy-start(bf16[896,2048]{1,0:T(8,128)(2,1)} %get-tuple-element.25) | copy-start | bytes 11010052
